TPU v7x, 32 devices: a whole 2x2x4 slice. The times are simulated.
32 devices in a mesh: sp: 4 (over z), fs: 4 (over y, x), tp: 2 (over core).
Axes of the slice: x: 2, y: 2, z: 4, core: 2. Of those that a mesh axis runs over, the one named last changes fastest.
Arguments:
- tokens: bfloat16 [4, 1024, 2048], P('fs', 'sp'), may hold values from -6 to 6
- mix_gain: float32 [2048], replicated, may hold values from 0.1 to 1.9
- query_down: bfloat16 [2048, 768], P('fs', 'tp'), may hold values from -0.125 to 0.125
- memory_down: bfloat16 [2048, 512], P('fs', 'tp'), may hold values from -0.125 to 0.125
- rope_weight: bfloat16 [2048, 32], replicated, may hold values from -0.125 to 0.125
- query_up: bfloat16 [768, 1536], P('fs', 'tp'), may hold values from -0.21875 to 0.21875
- key_up: bfloat16 [512, 1024], P('fs', 'tp'), may hold values from -0.25 to 0.25
- value_up: bfloat16 [512, 1024], P('fs', 'tp'), may hold values from -0.25 to 0.25
- latent_gain: float32 [768], replicated, may hold values from 0.1 to 1.9
- memory_gain: float32 [512], replicated, may hold values from 0.1 to 1.9
- query_gain: float32 [96], replicated, may hold values from 1 to 16
- key_gain: float32 [96], replicated, may hold values from 0.1 to 1.9
- conv_value: bfloat16 [2048, 1024], P('fs', 'tp'), may hold values from -1 to 1
- conv_gate: bfloat16 [2048, 1024], P('fs', 'tp'), may hold values from -0.125 to 0.125
- conv_kernel: bfloat16 [31, 1024], P(None, 'tp'), may hold values from -50 to 50
- channel_gain: float32 [1024], P('tp'), may hold values from 0.1 to 1.9
- channel_shift: float32 [1024], P('tp'), may hold values from -3 to 3
- heads_out: bfloat16 [1024, 2048], P('tp', 'fs'), may hold values from -0.75 to 0.75
- conv_out: bfloat16 [1024, 2048], P('tp', 'fs'), may hold values from -0.1875 to 0.1875
Outputs:
- mixed: bfloat16 [4, 1024, 2048], P('fs', 'sp')
All inputs are finite; a program needn't handle non-finite values.
Results may differ from a plain program's by a relative error of at most 0.015.
The roundings to bfloat16 on the way count: a program that leaves them out, or rounds other values in their place, can miss the bound.
Values may be sent and summed in bfloat16 or wider, within the bound.
A program may use at most 64 MiB of HBM per device.

v0:
```python
import functools

import jax
import jax.numpy as jnp
from jax import lax
from jax.experimental import pallas as pl
from jax.experimental.pallas import tpu as pltpu
from jax.sharding import PartitionSpec as P

MESH_ID = pl.DeviceIdType.MESH

QK_NOPE = 64
QK_ROPE = 32
V_DIM = 64
CONV_W = 1024
SEG = 64
QK_DIM = 96


epsilon = 1e-06
rope_base = 10000.0
masked_score = -1e30


def norm_rows(matrix, scale_vector):
    return (
        matrix
        * lax.rsqrt(jnp.mean(matrix * matrix, axis=-1, keepdims=True) + epsilon)
        * scale_vector
    )


def rope_tables(positions):
    inverse_freq = 1.0 / rope_base ** (jnp.arange(0, QK_ROPE, 2, dtype=jnp.float32) / QK_ROPE)
    angles = positions.astype(jnp.float32)[:, None] * inverse_freq[None, :]
    return (jnp.cos(angles)[:, None, :], jnp.sin(angles)[:, None, :])


def rotate(matrix, cosine_table, sine_table):
    half_width = matrix.shape[-1] // 2
    front_half = matrix[..., :half_width]
    back_half = matrix[..., half_width:]
    return jnp.concatenate(
        [
            front_half * cosine_table - back_half * sine_table,
            front_half * sine_table + back_half * cosine_table,
        ],
        axis=-1,
    )


def heads_query(latent, weight, scale_vector, cosine_table, sine_table):
    row_count = latent.shape[0]
    projected = jnp.dot(latent, weight, preferred_element_type=jnp.float32)
    projected = norm_rows(
        projected.reshape(row_count, weight.shape[1] // QK_DIM, QK_DIM), scale_vector
    )
    turned = rotate(projected[..., QK_NOPE:], cosine_table, sine_table)
    return jnp.concatenate([projected[..., :QK_NOPE], turned], axis=-1).astype(jnp.bfloat16)


def heads_key(latent, rope_rows, weight, scale_vector, cosine_table, sine_table):
    row_count = latent.shape[0]
    head_count = weight.shape[1] // QK_NOPE
    nope_part = jnp.dot(latent, weight, preferred_element_type=jnp.float32).reshape(
        row_count, head_count, QK_NOPE
    )
    shared = jnp.broadcast_to(
        rope_rows.astype(jnp.float32)[:, None, :], (row_count, head_count, QK_ROPE)
    )
    joined = norm_rows(jnp.concatenate([nope_part, shared], axis=-1), scale_vector)
    turned = rotate(joined[..., QK_NOPE:], cosine_table, sine_table)
    return jnp.concatenate([joined[..., :QK_NOPE], turned], axis=-1).astype(jnp.bfloat16)


RIM = 32


def relayed_rows(rows, paired):
    return (rows * 5 // 16) // 16 * 16 if paired else 0


def gather_kernel(
    sizes,
    x_ref, gain_ref, rope_ref, taps_ref, cgain_ref, cshift_ref,
    qd, md, cv, cg, qu, ku, vu, ho, co,
    lq_all, lm_all, rr_all, conv_ref, qu_all, ku_all, vu_all, ho_all, co_all,
    qd_all, md_all, cv_all, cg_all, normed, acc_q, acc_m, acc_v, acc_g, ext, tail, rim,
    sums, stats, stats_all,
    send_d, recv_d, send_r, recv_r, send_z, recv_z, local_sem, rim_sem,
    sp_send, sp_recv, rr_send, rr_recv, tp_send, tp_recv,
):
    n_fs, n_sp, n_tp = sizes
    paired = n_sp % 2 == 0
    f = lax.axis_index("fs")
    s = lax.axis_index("sp")
    t = lax.axis_index("tp")
    parity = lax.rem(s, 2)
    partner = s + 1 - 2 * parity

    barrier = pltpu.get_barrier_semaphore()
    for axis, at, count in (("fs", f, n_fs), ("sp", s, n_sp), ("tp", t, n_tp)):
        for k in range(1, count):
            pl.semaphore_signal(
                barrier, inc=1, device_id={axis: lax.rem(at + k, count)}, device_id_type=MESH_ID
            )
    pl.semaphore_wait(barrier, n_fs + n_sp + n_tp - 3)

    jobs = [
        (qd, qd_all, 0), (md, md_all, 0), (cv, cv_all, 0), (cg, cg_all, 0),
        (qu, qu_all, 0), (ku, ku_all, 0), (vu, vu_all, 0), (ho, ho_all, 1), (co, co_all, 1),
    ]
    last = len(jobs) - 1
    ahead = 4

    def place(whole, shard, dim, owner, start, count):
        rows, cols = shard.shape
        if dim == 0:
            return whole.at[pl.ds(pl.multiple_of(owner * rows + start, 16), count), :]
        return whole.at[
            pl.ds(pl.multiple_of(start, 16), count),
            pl.ds(pl.multiple_of(owner * cols, 128), cols),
        ]

    square = n_fs == 4
    if square:
        near_x = f + 1 - 2 * lax.rem(f, 2)
        near_y = lax.rem(f + 2, 4)
        far = lax.rem(near_x + 2, 4)
        targets = sources = [near_x, near_y]
    else:
        targets = [lax.rem(f + k, n_fs) for k in range(1, n_fs)]
        sources = [lax.rem(f + n_fs - k, n_fs) for k in range(1, n_fs)]

    direct, far_copies, over_sp, own = [], [], [], []
    for a, (shard, whole, dim) in enumerate(jobs):
        rows = shard.shape[0]
        less = 0 if a == last else relayed_rows(rows, paired)
        start = parity * less
        count = rows - less
        direct.append([
            pltpu.make_async_remote_copy(
                src_ref=shard.at[pl.ds(pl.multiple_of(start, 16), count), :],
                dst_ref=place(whole, shard, dim, f, start, count),
                send_sem=send_d.at[a, k], recv_sem=recv_d.at[a, k],
                device_id={"fs": target}, device_id_type=MESH_ID,
            )
            for k, target in enumerate(targets)
        ])
        halves = []
        if square:
            half = (count // 2 + 15) // 16 * 16
            for k, (owner, target, begin, size) in enumerate((
                (near_y, near_x, start, half), (near_x, near_y, start + half, count - half)
            )):
                piece = place(whole, shard, dim, owner, begin, size)
                halves.append(pltpu.make_async_remote_copy(
                    src_ref=piece, dst_ref=piece,
                    send_sem=send_r.at[a, k], recv_sem=recv_r.at[a, k],
                    device_id={"fs": target}, device_id_type=MESH_ID,
                ))
        far_copies.append(halves)
        across = []
        if less:
            lack = parity * (rows - less)
            for k, owner in enumerate(sources + ([far] if square else [])):
                piece = place(whole, shard, dim, owner, lack, less)
                across.append(pltpu.make_async_remote_copy(
                    src_ref=piece, dst_ref=piece,
                    send_sem=send_z.at[a, k], recv_sem=recv_z.at[a, k],
                    device_id={"sp": partner}, device_id_type=MESH_ID,
                ))
        over_sp.append(across)
        own.append(pltpu.make_async_copy(
            shard, place(whole, shard, dim, f, 0, rows), local_sem.at[a]
        ))

    def begin_array(a):
        if a <= last:
            for copy in direct[a]:
                copy.start()

    def finish_far(a):
        for copy in far_copies[a]:
            copy.wait_recv()
        for copy in over_sp[a][len(sources):]:
            copy.start()

    def tick(a):
        for copy in direct[a]:
            copy.wait_recv()
        for copy in far_copies[a]:
            copy.start()
        begin_array(a + ahead)
        for copy in over_sp[a][: len(sources)]:
            copy.start()
        if a >= 1:
            finish_far(a - 1)

    def complete(a):
        own[a].wait()
        for copy in over_sp[a]:
            copy.wait_recv()

    for a in range(ahead):
        begin_array(a)
    for copy in own:
        copy.start()

    rows = x_ref.shape[0]
    part = 32

    @pl.loop(0, rows // part)
    def _(i):
        at = pl.ds(pl.multiple_of(i * part, part), part)
        x = x_ref[at, :].astype(jnp.float32)
        scale = lax.rsqrt(jnp.mean(x * x, axis=-1, keepdims=True) + epsilon)
        normed[at, :] = (x * scale * gain_ref[...]).astype(jnp.bfloat16)

    depth = qd.shape[0]

    def project(weight, acc):
        acc[...] = jnp.zeros_like(acc)

        @pl.loop(0, n_fs)
        def _(i):
            at = pl.ds(pl.multiple_of(i * depth, depth), depth)
            acc[...] += jnp.dot(
                normed[:, at], weight[at, :], preferred_element_type=jnp.float32
            )

    mine = pl.ds(pl.multiple_of(s * rows, 16), rows)
    rr_all[mine, :] = jnp.dot(
        normed[...], rope_ref[...], preferred_element_type=jnp.float32
    ).astype(jnp.bfloat16)
    tick(0)
    tick(1)
    tick(2)
    complete(0)
    project(qd_all, acc_q)
    lq_all[t, :, :] = acc_q[...].astype(jnp.bfloat16)
    tick(3)
    complete(1)
    project(md_all, acc_m)
    lm_all[t, mine, :] = acc_m[...].astype(jnp.bfloat16)
    tick(4)
    complete(2)
    project(cv_all, acc_v)

    exchanges, passes = [], []
    for k in range(1, n_sp):
        peer = {"sp": lax.rem(s + k, n_sp)}
        exchanges.append(pltpu.make_async_remote_copy(
            src_ref=lm_all.at[t, mine, :], dst_ref=lm_all.at[t, mine, :],
            send_sem=sp_send.at[k - 1], recv_sem=sp_recv.at[k - 1],
            device_id=peer, device_id_type=MESH_ID,
        ))
        exchanges.append(pltpu.make_async_remote_copy(
            src_ref=rr_all.at[mine, :], dst_ref=rr_all.at[mine, :],
            send_sem=rr_send.at[k - 1], recv_sem=rr_recv.at[k - 1],
            device_id=peer, device_id_type=MESH_ID,
        ))
    tp_peers = [{"tp": lax.rem(t + k, n_tp)} for k in range(1, n_tp)]

    def to_tp(kind, source, landing):
        return [
            pltpu.make_async_remote_copy(
                src_ref=source, dst_ref=landing(k),
                send_sem=tp_send.at[kind, k], recv_sem=tp_recv.at[kind, k],
                device_id=peer, device_id_type=MESH_ID,
            )
            for k, peer in enumerate(tp_peers)
        ]

    query_copies = to_tp(0, lq_all.at[t], lambda k: lq_all.at[t])
    memory_copies = to_tp(1, lm_all.at[t], lambda k: lm_all.at[t])
    stat_copies = to_tp(2, stats, lambda k: stats_all.at[k])
    for copy in exchanges + query_copies:
        copy.start()
    tick(5)
    complete(3)
    project(cg_all, acc_g)

    @pl.loop(0, rows // part)
    def _(i):
        at = pl.ds(pl.multiple_of(i * part, part), part)
        gated = (acc_v[at, :] * jax.nn.sigmoid(acc_g[at, :])).astype(jnp.bfloat16)
        ext[pl.ds(pl.multiple_of(RIM + i * part, part), part), :] = gated.astype(jnp.float32)

    tail[...] = ext[pl.ds(rows, RIM), :].astype(jnp.bfloat16)
    rim_copy = pltpu.make_async_remote_copy(
        src_ref=tail, dst_ref=rim, send_sem=rim_sem.at[0], recv_sem=rim_sem.at[1],
        device_id={"sp": lax.rem(s + 1, n_sp)}, device_id_type=MESH_ID,
    )
    tick(6)

    @pl.when(s < n_sp - 1)
    def _():
        rim_copy.start()

    for copy in exchanges:
        copy.wait_recv()
    for copy in memory_copies:
        copy.start()

    @pl.when(s > 0)
    def _():
        rim_copy.wait_recv()
        ext[pl.ds(0, RIM), :] = rim[...].astype(jnp.float32)

    @pl.when(s == 0)
    def _():
        ext[pl.ds(0, RIM), :] = jnp.zeros((RIM, ext.shape[1]), jnp.float32)

    tap_count = taps_ref.shape[0]
    block = 64

    def convolve(c):
        cols = pl.ds(pl.multiple_of(c * 128, 128), 128)
        taps = taps_ref[:, cols].astype(jnp.float32)
        for r in range(0, rows, block):
            total = jnp.zeros((block, 128), jnp.float32)
            for j in range(tap_count):
                total = total + ext[
                    pl.ds(r + RIM - (tap_count - 1) + j, block), cols
                ] * taps[j : j + 1, :]
            sums[pl.ds(r, block), cols] = total

    tiles = ext.shape[1] // 128
    pl.loop(0, tiles // 2)(convolve)
    tick(7)
    pl.loop(tiles // 2, tiles)(convolve)

    @pl.loop(0, rows // part)
    def _(i):
        begin = pl.multiple_of(i * part, part)
        values = sums[pl.ds(begin, part), :]
        stats[pl.ds(begin, part), :] = jnp.broadcast_to(
            jnp.sum(values, axis=1, keepdims=True), (part, 128)
        )
        stats[pl.ds(pl.multiple_of(rows + begin, part), part), :] = jnp.broadcast_to(
            jnp.sum(values * values, axis=1, keepdims=True), (part, 128)
        )

    tick(8)
    for copy in stat_copies:
        copy.start()
    for copy in stat_copies:
        copy.wait_recv()

    channels = ext.shape[1] * n_tp

    @pl.loop(0, rows // part)
    def _(i):
        begin = pl.multiple_of(i * part, part)
        upper = pl.ds(begin, part)
        lower = pl.ds(pl.multiple_of(rows + begin, part), part)
        total, squares = stats[upper, :], stats[lower, :]
        for k in range(n_tp - 1):
            total = total + stats_all[k, upper, :]
            squares = squares + stats_all[k, lower, :]
        mean = total[:, :1] / channels
        spread = squares[:, :1] / channels - mean * mean
        shaped = (sums[upper, :] - mean) * lax.rsqrt(spread + epsilon)
        conv_ref[upper, :] = jax.nn.silu(
            shaped * cgain_ref[...] + cshift_ref[...]
        ).astype(jnp.bfloat16)

    finish_far(last)
    for a in range(4, last + 1):
        complete(a)
    for copy in query_copies + memory_copies:
        copy.wait_recv()
    for group in direct + far_copies + over_sp:
        for copy in group:
            copy.wait_send()
    for copy in exchanges + query_copies + memory_copies + stat_copies:
        copy.wait_send()

    @pl.when(s < n_sp - 1)
    def _():
        rim_copy.wait_send()


def gather_and_project(
    sizes, x, mix_gain, rope_weight, taps, channel_gain, channel_shift,
    qd, md, cv, cg, qu, ku, vu, ho, co,
):
    n_fs, n_sp, n_tp = sizes
    rows = x.shape[0]
    bf16, f32 = jnp.bfloat16, jnp.float32
    vmem = pl.BlockSpec(memory_space=pltpu.VMEM)
    hbm = pl.BlockSpec(memory_space=pl.ANY)

    def whole(w, dim=0):
        return (w.shape[0] * n_fs, w.shape[1]) if dim == 0 else (w.shape[0], w.shape[1] * n_fs)

    out_shapes = [
        ((n_tp, rows, qd.shape[1]), bf16), ((n_tp, n_sp * rows, md.shape[1]), bf16),
        ((n_sp * rows, rope_weight.shape[1]), bf16), ((rows, cv.shape[1]), bf16),
        (whole(qu), bf16), (whole(ku), bf16), (whole(vu), bf16),
        (whole(ho, 1), bf16), (whole(co, 1), bf16),
    ]
    dma = pltpu.SemaphoreType.DMA
    tp_others = max(n_tp - 1, 1)
    sp_others = max(n_sp - 1, 1)
    return pl.pallas_call(
        functools.partial(gather_kernel, sizes),
        out_shape=[jax.ShapeDtypeStruct(*o) for o in out_shapes],
        in_specs=[vmem] * 6 + [hbm] * 9,
        out_specs=[vmem] * 9,
        scratch_shapes=[
            pltpu.VMEM(whole(qd), bf16), pltpu.VMEM(whole(md), bf16),
            pltpu.VMEM(whole(cv), bf16), pltpu.VMEM(whole(cg), bf16),
            pltpu.VMEM(x.shape, bf16), pltpu.VMEM((rows, qd.shape[1]), f32),
            pltpu.VMEM((rows, md.shape[1]), f32),
            pltpu.VMEM((rows, cv.shape[1]), f32), pltpu.VMEM((rows, cv.shape[1]), f32),
            pltpu.VMEM((rows + RIM, cv.shape[1]), f32),
            pltpu.VMEM((RIM, cv.shape[1]), bf16), pltpu.VMEM((RIM, cv.shape[1]), bf16),
            pltpu.VMEM((rows, cv.shape[1]), f32), pltpu.VMEM((2 * rows, 128), f32),
            pltpu.VMEM((tp_others, 2 * rows, 128), f32),
            dma((9, n_fs - 1)), dma((9, n_fs - 1)), dma((9, 2)), dma((9, 2)),
            dma((9, n_fs - 1)), dma((9, n_fs - 1)), dma((9,)), dma((2,)),
            dma((sp_others,)), dma((sp_others,)), dma((sp_others,)), dma((sp_others,)),
            dma((3, tp_others)), dma((3, tp_others)),
        ],
        compiler_params=pltpu.CompilerParams(
            collective_id=0, has_side_effects=True, vmem_limit_bytes=56 * 1024 * 1024
        ),
    )(
        x, mix_gain[None, :], rope_weight, taps, channel_gain[None, :], channel_shift[None, :],
        qd, md, cv, cg, qu, ku, vu, ho, co,
    )


def key_block(key_count):
    block_size = key_count
    while block_size > 2048 and block_size % 2 == 0:
        block_size = block_size // 2
    return block_size


def sum_groups(partial):
    count = lax.axis_size("tp")
    if count != 2:
        return lax.psum(partial, "tp")
    other = lax.ppermute(partial, "tp", [(0, 1), (1, 0)])
    return (partial.astype(jnp.float32) + other.astype(jnp.float32)).astype(jnp.bfloat16)


def local(
    tokens,
    mix_gain,
    query_down,
    memory_down,
    rope_weight,
    query_up,
    key_up,
    value_up,
    latent_gain,
    memory_gain,
    query_gain,
    key_gain,
    conv_value,
    conv_gate,
    conv_kernel,
    channel_gain,
    channel_shift,
    heads_out,
    conv_out,
):
    own_rows = tokens[0]
    (
        query_parts, memory_parts, rope_piece, conv_result,
        up_query, up_keys, up_values, out_heads, out_conv,
    ) = gather_and_project(
        (lax.axis_size("fs"), lax.axis_size("sp"), lax.axis_size("tp")),
        own_rows, mix_gain, rope_weight, conv_kernel, channel_gain, channel_shift,
        query_down, memory_down, conv_value, conv_gate,
        query_up, key_up, value_up, heads_out, conv_out,
    )
    row_count = own_rows.shape[0]
    whole_query = jnp.concatenate(list(query_parts), axis=1)
    whole_memory = jnp.concatenate(list(memory_parts), axis=1)
    query_normed = norm_rows(whole_query.astype(jnp.float32), latent_gain).astype(jnp.bfloat16)
    memory_piece = norm_rows(whole_memory.astype(jnp.float32), memory_gain).astype(jnp.bfloat16)
    positions = lax.axis_index("sp") * row_count + jnp.arange(row_count, dtype=jnp.int32)
    cosine_table, sine_table = rope_tables(positions)
    queries = heads_query(query_normed, up_query, query_gain, cosine_table, sine_table)
    head_count = queries.shape[1]
    query_segment = positions // SEG
    score_scale = QK_DIM ** (-0.5)
    def attend(state_carry, key_rows, value_rows, key_pos):
        running_max, row_total, weighted = state_carry
        scores = (
            jnp.einsum("qhd,khd->qhk", queries, key_rows, preferred_element_type=jnp.float32)
            * score_scale
        )
        allowed = ((key_pos // SEG)[None, :] <= query_segment[:, None])[:, None, :]
        scores = jnp.where(allowed, scores, masked_score)
        new_max = jnp.maximum(running_max, jnp.max(scores, axis=2))
        weights = jnp.where(allowed, jnp.exp(scores - new_max[:, :, None]), 0.0)
        factor = jnp.exp(running_max - new_max)
        row_total = row_total * factor + jnp.sum(weights, axis=2)
        weighted = weighted * factor[:, :, None] + jnp.einsum(
            "qhk,khd->qhd",
            weights.astype(jnp.bfloat16),
            value_rows,
            preferred_element_type=jnp.float32,
        )
        return (new_max, row_total, weighted)

    initial = (
        jnp.full((row_count, head_count), masked_score, jnp.float32),
        jnp.zeros((row_count, head_count), jnp.float32),
        jnp.zeros((row_count, head_count, V_DIM), jnp.float32),
    )
    def block_keys(block_start, block_size):
        memory_block = lax.dynamic_slice_in_dim(memory_piece, block_start, block_size, 0)
        rope_block = lax.dynamic_slice_in_dim(rope_piece, block_start, block_size, 0)
        key_pos = block_start + jnp.arange(block_size, dtype=jnp.int32)
        cosine_keys, sine_keys = rope_tables(key_pos)
        key_rows = heads_key(memory_block, rope_block, up_keys, key_gain, cosine_keys, sine_keys)
        value_rows = (
            jnp.dot(memory_block, up_values, preferred_element_type=jnp.float32)
            .astype(jnp.bfloat16)
            .reshape(block_size, head_count, V_DIM)
        )
        return (key_rows, value_rows, key_pos)

    key_count = memory_piece.shape[0]
    block_size = key_block(key_count)

    def step(block_index, running):
        key_rows, value_rows, key_pos = block_keys(block_index * block_size, block_size)
        return attend(running, key_rows, value_rows, key_pos)

    final_state = lax.fori_loop(0, key_count // block_size, step, initial)
    running_max, row_total, weighted = final_state
    attention = (
        (weighted / row_total[:, :, None])
        .astype(jnp.bfloat16)
        .reshape(row_count, head_count * V_DIM)
    )
    mixer_rows = jnp.concatenate([attention, conv_result], axis=1)
    out_weight = jnp.concatenate([out_heads, out_conv], axis=0)
    partial_sum = jnp.dot(mixer_rows, out_weight, preferred_element_type=jnp.float32)
    mixed = sum_groups(partial_sum.astype(jnp.bfloat16))
    return mixed[None]


def solution(mesh):
    in_specs = (
        P("fs", "sp", None),
        P(),
        P("fs", "tp"),
        P("fs", "tp"),
        P(),
        P("fs", "tp"),
        P("fs", "tp"),
        P("fs", "tp"),
        P(),
        P(),
        P(),
        P(),
        P("fs", "tp"),
        P("fs", "tp"),
        P(None, "tp"),
        P("tp"),
        P("tp"),
        P("tp", "fs"),
        P("tp", "fs"),
    )
    out_specs = P("fs", "sp", None)
    return jax.shard_map(local, mesh=mesh, in_specs=in_specs, out_specs=out_specs, check_vma=False)
```

profile of v0, /device:TPU:0, one launch (start us, length us, event | category | flops | bytes accessed | tf_op | source)
XLA Modules:
  0.0 125.4 jit_solution(11487985203968246603)
XLA Ops:
  0.0 0.1 multiply_cosine_fusion.1
  0.2 0.3 multiply_cosine_fusion
  0.5 1.9 %copy.25.rope_ref = bf16[2048,32]{1,0:T(8,128)(2,1)} copy(bf16[2048,32]{0,1:T(8,128)(2,1)} %param.23) | data formatting | bytes 262144 | tf_op args[4]
  2.4 103.0 %shard_map.181 = (bf16[2,256,384]{2,1,0:T(8,128)(2,1)}, bf16[2,1024,256]{2,1,0:T(8,128)(2,1)}, bf16[1024,32]{1,0:T(8,128)(2,1)}, bf16[256,512]{1,0:T(8,128)(2,1)...) custom-call(bf16[256,2048]{1,0:T(8,128)(2,1)} %bitcast.53, ...), custom_call_target="tpu_custom_call" | custom-call | tf_op jit(solution)/shard_map/pallas_call | solution.py:407
  105.4 0.0 copy-start.9
  105.4 1.4 %slice_bitcast_fusion.1 = (bf16[1024,256]{1,0:T(8,128)(2,1)S(1)}, bf16[1024,256]{1,0:T(8,128)(2,1)S(1)}) fusion(bf16[2,1024,256]{2,1,0:T(8,128)(2,1)} %get-tuple-element.48), kind=kLoop, calls=%fused_computation.49 | loop fusion | bytes 2097152 | tf_op jit(solution)/shard_map/unstack | solution.py:484
  106.8 0.0 copy-start.2
  106.8 0.3 fusion.13
  107.1 0.1 copy.26
  107.3 0.0 copy-start.10
  107.3 0.2 fusion.35
  107.5 0.6 fusion.41
  108.2 0.1 multiply_reduce_fusion.1
  108.3 0.1 multiply_multiply_fusion.1
  108.5 0.9 convolution_convert_fusion
  109.4 0.9 fusion.62
  110.3 0.0 copy-start.3
  110.3 0.1 broadcast_in_dim.91
  110.5 0.4 multiply_reduce_fusion
  110.9 0.1 copy-done.3
  111.0 0.6 multiply_multiply_fusion
  111.6 0.2 slice.52
  111.8 0.2 broadcast_compare_fusion
  112.0 0.1 subtract_convert_fusion
  112.2 1.7 %fusion = (f32[256,8]{0,1:T(8,128)S(1)}, f32[8,1024,256]{2,1,0:T(8,128)S(1)}) fusion(pred[256,1024]{0,1:T(8,128)(4,1)S(1)} %broadcast_compare_fusion, bf16[256,8,16]{0,2,1:T(8,128)(2,1)S(1)} %get-tuple-element.64, bf16[256,8,16]{0,2,1:T(8,128)(2,1)S(1)} %get-tuple-element.63, bf16[256,8,64]{0,2,1:T(8,128)(2,1)S(1)} %slice.53, ...), kind=kOutput, calls=%fused_computation.2 | convolution fusion | flops 414840832 | bytes 10625024 | tf_op jit(solution)/shard_map/while/body/eval_jaxpr/qhd,khd->qhk/dot_general | solution.py:496
  113.9 2.2 %fusion.1 = f32[256,8]{0,1:T(8,128)S(1)} fusion(f32[8,1024,256]{2,1,0:T(8,128)S(1)} %get-tuple-element.74, f32[256,8]{0,1:T(8,128)S(1)} %broadcast_maximum_fusion, pred[256,1024]{0,1:T(8,128)(4,1)S(1)} %broadcast_compare_fusion), kind=kLoop, calls=%fused_computation.3 | loop fusion | flops 10483712 | bytes 8667136 | tf_op jit(solution)/shard_map/while/body/eval_jaxpr/reduce_sum | solution.py:504
  116.1 2.2 %fusion.32 = bf16[256,8,64]{0,2,1:T(8,128)(2,1)S(1)} fusion(bf16[1024,8,64]{0,2,1:T(8,128)(2,1)S(1)} %bitcast.58, f32[8,1024,256]{2,1,0:T(8,128)S(1)} %get-tuple-element.74, f32[256,8]{0,1:T(8,128)S(1)} %broadcast_maximum_fusion, pred[256,1024]{0,1:T(8,128)(4,1)S(1)} %broadcast_compare_fusion, f32[256,8]{0,1:T(8,128)S(1)} %get-tuple-element.68, ...), kind=kOutput, calls=%fused_computation.34 | convolution fusion | flops 279314432 | bytes 9986048 | tf_op jit(solution)/shard_map/while/body/eval_jaxpr/qhk,khd->qhd/dot_general | solution.py:505
  118.3 0.1 copy.29
  118.5 2.8 %fusion.10 = bf16[256,2048]{1,0:T(8,128)(2,1)S(1)} fusion(bf16[512,2048]{1,0:T(8,128)(2,1)} %get-tuple-element.58, bf16[512,2048]{1,0:T(8,128)(2,1)S(1)} %copy-done.4, bf16[256,512]{1,0:T(8,128)(2,1)S(1)} %copy-done.8, bf16[256,512]{1,0:T(8,128)(2,1)S(1)} %copy.29), kind=kOutput, calls=%fused_computation.16 | convolution fusion | flops 1083703296 | bytes 5767168 | tf_op jit(solution)/shard_map/dot_general | solution.py:547
  121.3 0.1 collective-permute-start
  121.4 2.6 %collective-permute-done = bf16[256,2048]{1,0:T(8,128)(2,1)S(1)} collective-permute-done((bf16[256,2048]{1,0:T(8,128)(2,1)S(1)}, bf16[256,2048]{1,0:T(8,128)(2,1)S(1)}, u32[]{:S(2)}, u32[]{:S(2)}) %collective-permute-start) | collective-permute-done | bytes 1048608 | tf_op jit(solution)/shard_map/ppermute | solution.py:447
  124.1 1.4 %fusion.28 = bf16[1,256,2048]{2,1,0:T(8,128)(2,1)} fusion(bf16[256,2048]{1,0:T(8,128)(2,1)S(1)} %collective-permute-done, bf16[256,2048]{1,0:T(8,128)(2,1)S(1)} %fusion.10), kind=kLoop, calls=%fused_computation.31 | loop fusion | flops 2097152 | bytes 3145728 | tf_op jit(solution)/shard_map/broadcast_in_dim | solution.py:549
  (30 shorter events, 0.2 us)
Async XLA Ops:
  105.4 1.7 %copy-start.1 = (bf16[1024,32]{1,0:T(8,128)(2,1)S(1)}, bf16[1024,32]{1,0:T(8,128)(2,1)}, u32[]{:S(2)}) copy-start(bf16[1024,32]{1,0:T(8,128)(2,1)} %get-tuple-element.52) | copy-start | bytes 196612
  105.4 1.9 %copy-start = (bf16[2,256,384]{2,1,0:T(8,128)(2,1)S(1)}, bf16[2,256,384]{2,1,0:T(8,128)(2,1)}, u32[]{:S(2)}) copy-start(bf16[2,256,384]{2,1,0:T(8,128)(2,1)} %get-tuple-element.53) | copy-start | bytes 1179652
  105.4 2.1 %copy-start.5 = (bf16[768,768]{1,0:T(8,128)(2,1)S(1)}, bf16[768,768]{1,0:T(8,128)(2,1)}, u32[]{:S(2)}) copy-start(bf16[768,768]{1,0:T(8,128)(2,1)} %get-tuple-element.54) | copy-start | bytes 3538948
  105.4 2.1 %copy-start.9 = (f32[768]{0:T(1024)S(1)}, f32[768]{0:T(1024)}, u32[]{:S(2)}) copy-start(f32[768]{0:T(1024)} %param.27) | copy-start | bytes 9220
  106.8 1.4 %copy-start.2 = (f32[96]{0:T(128)S(1)}, f32[96]{0:T(128)}, u32[]{:S(2)}) copy-start(f32[96]{0:T(128)} %param.29) | copy-start | bytes 1156
  107.3 1.2 copy-start.7
  107.3 1.2 copy-start.10
  108.3 1.1 copy-start.6
  110.3 0.7 copy-start.3
  116.1 2.4 %copy-start.4 = (bf16[512,2048]{1,0:T(8,128)(2,1)S(1)}, bf16[512,2048]{1,0:T(8,128)(2,1)}, u32[]{:S(2)}) copy-start(bf16[512,2048]{1,0:T(8,128)(2,1)} %get-tuple-element.57) | copy-start | bytes 6291460
  116.1 2.4 %copy-start.8 = (bf16[256,512]{1,0:T(8,128)(2,1)S(1)}, bf16[256,512]{1,0:T(8,128)(2,1)}, u32[]{:S(2)}) copy-start(bf16[256,512]{1,0:T(8,128)(2,1)} %get-tuple-element.56) | copy-start | bytes 786436
  121.3 2.7 %collective-permute-start = (bf16[256,2048]{1,0:T(8,128)(2,1)S(1)}, bf16[256,2048]{1,0:T(8,128)(2,1)S(1)}, u32[]{:S(2)}, u32[]{:S(2)}) collective-permute-start(bf16[256,2048]{1,0:T(8,128)(2,1)S(1)} %fusion.10), channel_id=1, source_target_pairs={{0,1},{1,0},{2,3},{3,2},{4,5},{5,4},{6,7},{7,6},{8,9},{9,8},{10,11... | collective-permute-start | bytes 3145736 | tf_op jit(solution)/shard_map/ppermute | solution.py:447
where the time goes:
time: 126 us; the launch traced here: 125 us
  Pallas kernels  103 us (82%)
  matrix products  9.17 us (7%)
  other arithmetic  6.13 us (5%)
  local copies, waits for them, and re-layouts  4.04 us (3%)
  waiting for transfers between devices  2.65 us (2%)
    pallas_call x1, Pallas kernels, gather_and_project(): pl.pallas_call(functools.partial(gather_kernel, sizes), out_shape=[jax.Sh...  103 us
    dot_general x1, matrix products, local(): jnp.dot(mixer_rows, out_weight, preferred_element_type=jnp.float32)  2.84 us
    ppermute x1, waiting for transfers between devices, sum_groups(): other = lax.ppermute(partial, 'tp', [(0, 1), (1, 0)])  2.65 us
  transfers between devices with their start and end apart: 1, of which 1 were waited for; matrix products, arithmetic and copies ran while one was open for 0% of the time, Pallas kernels for 0%

commit v1 on v0

--- a/solution.py
+++ b/solution.py
@@ -2,6 +2,7 @@
 
 import jax
 import jax.numpy as jnp
+import numpy as np
 from jax import lax
 from jax.experimental import pallas as pl
 from jax.experimental.pallas import tpu as pltpu
@@ -549,6 +550,539 @@
     return mixed[None]
 
 
+def table_rows(count):
+    inverse_freq = 1.0 / np.float32(rope_base) ** (
+        np.arange(0, QK_ROPE, 2, dtype=np.float32) / np.float32(QK_ROPE)
+    )
+    angles = inverse_freq[:, None] * np.arange(count, dtype=np.float32)[None, :]
+    angles = angles.astype(np.float64)
+    return np.cos(angles).astype(np.float32), np.sin(angles).astype(np.float32)
+
+
+def dot_heads(left, right):
+    return lax.dot_general(
+        left, right, (((0,), (0,)), ((), ())), preferred_element_type=jnp.float32
+    )
+
+
+def fused_kernel(
+    sizes,
+    x_ref, gain_ref, rope_ref, taps_ref, cgain_ref, cshift_ref,
+    lgain_ref, mgain_ref, qgain_ref, kgain_ref, cos_ref, sin_ref,
+    md, qd, ku, vu, qu, cv, cg, ho, co,
+    mine_ref, other_ref,
+    md_all, qd_all, ku_all, vu_all, qu_all, cv_all, cg_all, ho_all, co_all,
+    normed, lq_all, lm_all, mem_all, rr_all, qn_t, q_t, k_t, v_t, turned, ropesq, bias, scores,
+    att_t, conv_s, acc_v, acc_g, acc_out, ext, tail, rim, sums, stats, stats_all,
+    send_d, recv_d, send_r, recv_r, send_z, recv_z, local_sem, rim_sem,
+    sp_send, sp_recv, rr_send, rr_recv, fw_send, fw_recv, tp_send, tp_recv, out_send, out_recv,
+):
+    n_fs, n_sp, n_tp = sizes
+    f = lax.axis_index("fs")
+    s = lax.axis_index("sp")
+    t = lax.axis_index("tp")
+    parity = lax.rem(s, 2)
+    partner = s + 1 - 2 * parity
+    twin = {"tp": 1 - t}
+
+    barrier = pltpu.get_barrier_semaphore()
+    for axis, at, count in (("fs", f, n_fs), ("sp", s, n_sp), ("tp", t, n_tp)):
+        for k in range(1, count):
+            pl.semaphore_signal(
+                barrier, inc=1, device_id={axis: lax.rem(at + k, count)}, device_id_type=MESH_ID
+            )
+    pl.semaphore_wait(barrier, n_fs + n_sp + n_tp - 3)
+
+    jobs = [
+        (md, md_all, 0), (qd, qd_all, 0), (ku, ku_all, 0), (vu, vu_all, 0), (qu, qu_all, 0),
+        (cv, cv_all, 0), (cg, cg_all, 0), (ho, ho_all, 1), (co, co_all, 1),
+    ]
+    last = len(jobs) - 1
+    ahead = 4
+
+    def place(whole, shard, dim, owner, start, count):
+        rows, cols = shard.shape
+        if dim == 0:
+            return whole.at[pl.ds(pl.multiple_of(owner * rows + start, 16), count), :]
+        return whole.at[
+            pl.ds(pl.multiple_of(start, 16), count),
+            pl.ds(pl.multiple_of(owner * cols, 128), cols),
+        ]
+
+    near_x = f + 1 - 2 * lax.rem(f, 2)
+    near_y = lax.rem(f + 2, 4)
+    far = lax.rem(near_x + 2, 4)
+    sources = [near_x, near_y]
+
+    direct, far_copies, over_sp, own = [], [], [], []
+    for a, (shard, whole, dim) in enumerate(jobs):
+        rows = shard.shape[0]
+        less = 0 if a == last else relayed_rows(rows, True)
+        start = parity * less
+        count = rows - less
+        direct.append([
+            pltpu.make_async_remote_copy(
+                src_ref=shard.at[pl.ds(pl.multiple_of(start, 16), count), :],
+                dst_ref=place(whole, shard, dim, f, start, count),
+                send_sem=send_d.at[a, k], recv_sem=recv_d.at[a, k],
+                device_id={"fs": target}, device_id_type=MESH_ID,
+            )
+            for k, target in enumerate(sources)
+        ])
+        halves = []
+        half = (count // 2 + 15) // 16 * 16
+        for k, (owner, target, begin, size) in enumerate((
+            (near_y, near_x, start, half), (near_x, near_y, start + half, count - half)
+        )):
+            piece = place(whole, shard, dim, owner, begin, size)
+            halves.append(pltpu.make_async_remote_copy(
+                src_ref=piece, dst_ref=piece,
+                send_sem=send_r.at[a, k], recv_sem=recv_r.at[a, k],
+                device_id={"fs": target}, device_id_type=MESH_ID,
+            ))
+        far_copies.append(halves)
+        across = []
+        if less:
+            lack = parity * (rows - less)
+            for k, owner in enumerate(sources + [far]):
+                piece = place(whole, shard, dim, owner, lack, less)
+                across.append(pltpu.make_async_remote_copy(
+                    src_ref=piece, dst_ref=piece,
+                    send_sem=send_z.at[a, k], recv_sem=recv_z.at[a, k],
+                    device_id={"sp": partner}, device_id_type=MESH_ID,
+                ))
+        over_sp.append(across)
+        own.append(pltpu.make_async_copy(
+            shard, place(whole, shard, dim, f, 0, rows), local_sem.at[a]
+        ))
+
+    def begin_array(a):
+        if a <= last:
+            for copy in direct[a]:
+                copy.start()
+
+    def finish_far(a):
+        for copy in far_copies[a]:
+            copy.wait_recv()
+        for copy in over_sp[a][len(sources):]:
+            copy.start()
+
+    def tick(a):
+        for copy in direct[a]:
+            copy.wait_recv()
+        for copy in far_copies[a]:
+            copy.start()
+        begin_array(a + ahead)
+        for copy in over_sp[a][: len(sources)]:
+            copy.start()
+        if a >= 1:
+            finish_far(a - 1)
+
+    def complete(a):
+        own[a].wait()
+        for copy in over_sp[a]:
+            copy.wait_recv()
+
+    for a in range(ahead):
+        begin_array(a)
+    for copy in own:
+        copy.start()
+
+    rows = x_ref.shape[0]
+    part = 32
+
+    @pl.loop(0, rows // part)
+    def _(i):
+        at = pl.ds(pl.multiple_of(i * part, part), part)
+        x = x_ref[at, :].astype(jnp.float32)
+        scale = lax.rsqrt(jnp.mean(x * x, axis=-1, keepdims=True) + epsilon)
+        normed[at, :] = (x * scale * gain_ref[...]).astype(jnp.bfloat16)
+
+    depth = qd.shape[0]
+
+    def project(weight, acc):
+        acc[...] = jnp.zeros_like(acc)
+
+        @pl.loop(0, n_fs)
+        def _(i):
+            at = pl.ds(pl.multiple_of(i * depth, depth), depth)
+            acc[...] += jnp.dot(
+                normed[:, at], weight[at, :], preferred_element_type=jnp.float32
+            )
+
+    rr_all[s] = lax.dot_general(
+        rope_ref[...], normed[...], (((1,), (1,)), ((), ())), preferred_element_type=jnp.float32
+    ).astype(jnp.bfloat16)
+
+    half_rope = QK_ROPE // 2
+
+    @pl.loop(s + 1, n_sp)
+    def _(j):
+        mem_all[j] = jnp.zeros(mem_all.shape[1:], jnp.bfloat16)
+        rr_all[j] = jnp.zeros(rr_all.shape[1:], jnp.bfloat16)
+
+    @pl.loop(0, n_sp)
+    def _(j):
+        key_at = j * rows + lax.broadcasted_iota(jnp.int32, (rows, rows), 0)
+        query_at = s * rows + lax.broadcasted_iota(jnp.int32, (rows, rows), 1)
+        bias[j] = jnp.where(
+            lax.div(key_at, SEG) <= lax.div(query_at, SEG), 0.0, masked_score
+        )
+
+    def to_twin(kind, source, landing):
+        return pltpu.make_async_remote_copy(
+            src_ref=source, dst_ref=landing,
+            send_sem=tp_send.at[kind], recv_sem=tp_recv.at[kind],
+            device_id=twin, device_id_type=MESH_ID,
+        )
+
+    query_copy = to_twin(0, lq_all.at[t], lq_all.at[t])
+    memory_copy = to_twin(1, lm_all.at[t], lm_all.at[t])
+    stat_copy = to_twin(2, stats, stats_all)
+
+    lat = md.shape[1]
+    held = pl.ds(pl.multiple_of(t * lat, lat), lat)
+    sends, forwards = [], []
+    for k in range(1, n_sp):
+        peer = {"sp": lax.rem(s + k, n_sp)}
+        sends.append([
+            pltpu.make_async_remote_copy(
+                src_ref=mem_all.at[s, held, :], dst_ref=mem_all.at[s, held, :],
+                send_sem=sp_send.at[k - 1], recv_sem=sp_recv.at[k - 1],
+                device_id=peer, device_id_type=MESH_ID,
+            ),
+            pltpu.make_async_remote_copy(
+                src_ref=rr_all.at[s], dst_ref=rr_all.at[s],
+                send_sem=rr_send.at[k - 1], recv_sem=rr_recv.at[k - 1],
+                device_id=peer, device_id_type=MESH_ID,
+            ),
+        ])
+        behind = mem_all.at[lax.rem(s + n_sp - k, n_sp), held, :]
+        forwards.append(pltpu.make_async_remote_copy(
+            src_ref=behind, dst_ref=behind,
+            send_sem=fw_send.at[k - 1], recv_sem=fw_recv.at[k - 1],
+            device_id=twin, device_id_type=MESH_ID,
+        ))
+
+    tick(0)
+    tick(1)
+    tick(2)
+    complete(0)
+    project(md_all, acc_v.at[:, pl.ds(0, lat)])
+    lm_all[t, :, :] = acc_v[:, :lat].astype(jnp.bfloat16)
+    memory_copy.start()
+    tick(3)
+    complete(1)
+    wide = qd.shape[1]
+    project(qd_all, acc_g.at[:, pl.ds(0, wide)])
+    lq_all[t, :, :] = acc_g[:, :wide].astype(jnp.bfloat16)
+    query_copy.start()
+
+    def normed_columns(parts, gains, put):
+        width = parts.shape[2]
+
+        @pl.loop(0, rows // 128)
+        def _(i):
+            at = pl.ds(pl.multiple_of(i * 128, 128), 128)
+            pieces = [parts[g, at, :].astype(jnp.float32) for g in range(n_tp)]
+            total = sum(jnp.sum(p * p, axis=-1, keepdims=True) for p in pieces)
+            scale = lax.rsqrt(total / (width * n_tp) + epsilon)
+            for g in range(n_tp):
+                gain = gains[:, g * width : (g + 1) * width]
+                shaped = (pieces[g] * scale * gain).astype(jnp.bfloat16)
+                put(g * width, width, at, shaped.astype(jnp.float32).T.astype(jnp.bfloat16))
+
+    def put_memory(begin, width, at, piece):
+        mem_all[s, begin : begin + width, at] = piece
+
+    def put_query(begin, width, at, piece):
+        qn_t[begin : begin + width, at] = piece
+
+    memory_copy.wait_recv()
+    normed_columns(lm_all, mgain_ref, put_memory)
+    for k in range(1, n_sp):
+        @pl.when(s + k < n_sp)
+        def _(k=k):
+            for copy in sends[k - 1]:
+                copy.start()
+
+    tick(4)
+    query_copy.wait_recv()
+    normed_columns(lq_all, lgain_ref, put_query)
+    complete(2)
+    tick(5)
+    complete(3)
+
+    for k in range(1, n_sp):
+        @pl.when(s >= k)
+        def _(k=k):
+            for copy in sends[k - 1]:
+                copy.wait_recv()
+            forwards[k - 1].start()
+    for k in range(1, n_sp):
+        @pl.when(s >= k)
+        def _(k=k):
+            forwards[k - 1].wait_recv()
+
+    @pl.loop(0, n_sp)
+    def _(j):
+        k_t[j] = dot_heads(ku_all[...], mem_all[j])
+        v_t[j] = dot_heads(vu_all[...], mem_all[j]).astype(jnp.bfloat16)
+        shared = rr_all[j].astype(jnp.float32)
+        ropesq[j] = jnp.sum(shared * shared, axis=0, keepdims=True)
+        shared = shared * kgain_ref[QK_NOPE:, :]
+        front, back = shared[:half_rope], shared[half_rope:]
+        at = pl.ds(pl.multiple_of(j * rows, rows), rows)
+        cosine, sine = cos_ref[:, at], sin_ref[:, at]
+        turned[j] = jnp.concatenate(
+            [front * cosine - back * sine, front * sine + back * cosine], axis=0
+        )
+
+    tick(6)
+    complete(4)
+    q_t[...] = dot_heads(qu_all[...], qn_t[...])
+    heads = qu.shape[1] // QK_DIM
+    here = pl.ds(pl.multiple_of(s * rows, rows), rows)
+    score_scale = QK_DIM ** (-0.5)
+
+    def head(h):
+        q = q_t[pl.ds(pl.multiple_of(h * QK_DIM, QK_DIM), QK_DIM), :]
+        q = q * lax.rsqrt(jnp.mean(q * q, axis=0, keepdims=True) + epsilon) * qgain_ref[...]
+        front, back = q[QK_NOPE : QK_NOPE + half_rope], q[QK_NOPE + half_rope :]
+        cosine, sine = cos_ref[:, here], sin_ref[:, here]
+        q = jnp.concatenate(
+            [q[:QK_NOPE], front * cosine - back * sine, front * sine + back * cosine], axis=0
+        ).astype(jnp.bfloat16)
+        krow = pl.ds(pl.multiple_of(h * QK_NOPE, QK_NOPE), QK_NOPE)
+        vrow = pl.ds(pl.multiple_of(h * V_DIM, V_DIM), V_DIM)
+        top = jnp.full((1, rows), masked_score, jnp.float32)
+        for j in range(n_sp):
+            nope = k_t[j, krow, :]
+            scale = lax.rsqrt(
+                (jnp.sum(nope * nope, axis=0, keepdims=True) + ropesq[j]) / QK_DIM + epsilon
+            )
+            key = jnp.concatenate(
+                [nope * scale * kgain_ref[:QK_NOPE, :], turned[j] * scale], axis=0
+            ).astype(jnp.bfloat16)
+            block = dot_heads(key, q) + bias[j]
+            scores[j] = block
+            top = jnp.maximum(top, jnp.max(block, axis=0, keepdims=True))
+        total = jnp.zeros((1, rows), jnp.float32)
+        summed = jnp.zeros((V_DIM, rows), jnp.float32)
+        for j in range(n_sp):
+            weight = jnp.exp((scores[j] - top) * score_scale)
+            total = total + jnp.sum(weight, axis=0, keepdims=True)
+            summed = summed + jnp.dot(
+                v_t[j, vrow, :], weight.astype(jnp.bfloat16),
+                preferred_element_type=jnp.float32,
+            )
+        att_t[vrow, :] = summed / total
+
+    pl.loop(0, heads // 2)(head)
+    tick(7)
+    pl.loop(heads // 2, heads)(head)
+    complete(5)
+    project(cv_all, acc_v)
+    tick(8)
+    complete(6)
+    project(cg_all, acc_g)
+
+    @pl.loop(0, rows // part)
+    def _(i):
+        at = pl.ds(pl.multiple_of(i * part, part), part)
+        gated = (acc_v[at, :] * jax.nn.sigmoid(acc_g[at, :])).astype(jnp.bfloat16)
+        ext[pl.ds(pl.multiple_of(RIM + i * part, part), part), :] = gated.astype(jnp.float32)
+
+    tail[...] = ext[pl.ds(rows, RIM), :].astype(jnp.bfloat16)
+    rim_copy = pltpu.make_async_remote_copy(
+        src_ref=tail, dst_ref=rim, send_sem=rim_sem.at[0], recv_sem=rim_sem.at[1],
+        device_id={"sp": lax.rem(s + 1, n_sp)}, device_id_type=MESH_ID,
+    )
+
+    @pl.when(s < n_sp - 1)
+    def _():
+        rim_copy.start()
+
+    @pl.when(s > 0)
+    def _():
+        rim_copy.wait_recv()
+        ext[pl.ds(0, RIM), :] = rim[...].astype(jnp.float32)
+
+    @pl.when(s == 0)
+    def _():
+        ext[pl.ds(0, RIM), :] = jnp.zeros((RIM, ext.shape[1]), jnp.float32)
+
+    tap_count = taps_ref.shape[0]
+    block = 64
+
+    def convolve(c):
+        cols = pl.ds(pl.multiple_of(c * 128, 128), 128)
+        taps = taps_ref[:, cols].astype(jnp.float32)
+        for r in range(0, rows, block):
+            total = jnp.zeros((block, 128), jnp.float32)
+            for j in range(tap_count):
+                total = total + ext[
+                    pl.ds(r + RIM - (tap_count - 1) + j, block), cols
+                ] * taps[j : j + 1, :]
+            sums[pl.ds(r, block), cols] = total
+
+    tiles = ext.shape[1] // 128
+    pl.loop(0, tiles)(convolve)
+    finish_far(last)
+
+    @pl.loop(0, rows // part)
+    def _(i):
+        begin = pl.multiple_of(i * part, part)
+        values = sums[pl.ds(begin, part), :]
+        stats[pl.ds(begin, part), :] = jnp.broadcast_to(
+            jnp.sum(values, axis=1, keepdims=True), (part, 128)
+        )
+        stats[pl.ds(pl.multiple_of(rows + begin, part), part), :] = jnp.broadcast_to(
+            jnp.sum(values * values, axis=1, keepdims=True), (part, 128)
+        )
+
+    stat_copy.start()
+    complete(7)
+    att = att_t[...].T.astype(jnp.bfloat16)
+    span = ho.shape[1]
+
+    @pl.loop(0, n_fs)
+    def _(i):
+        cols = pl.ds(pl.multiple_of(i * span, span), span)
+        acc_out[:, cols] = jnp.dot(att, ho_all[:, cols], preferred_element_type=jnp.float32)
+
+    stat_copy.wait_recv()
+    channels = ext.shape[1] * n_tp
+
+    @pl.loop(0, rows // part)
+    def _(i):
+        begin = pl.multiple_of(i * part, part)
+        upper = pl.ds(begin, part)
+        lower = pl.ds(pl.multiple_of(rows + begin, part), part)
+        total = stats[upper, :] + stats_all[upper, :]
+        squares = stats[lower, :] + stats_all[lower, :]
+        mean = total[:, :1] / channels
+        spread = squares[:, :1] / channels - mean * mean
+        shaped = (sums[upper, :] - mean) * lax.rsqrt(spread + epsilon)
+        conv_s[upper, :] = jax.nn.silu(
+            shaped * cgain_ref[...] + cshift_ref[...]
+        ).astype(jnp.bfloat16)
+
+    complete(8)
+    outs = []
+    for i in range(n_fs):
+        cols = slice(i * span, (i + 1) * span)
+        outs.append(pltpu.make_async_remote_copy(
+            src_ref=mine_ref.at[:, cols], dst_ref=other_ref.at[:, cols],
+            send_sem=out_send.at[i], recv_sem=out_recv.at[i],
+            device_id=twin, device_id_type=MESH_ID,
+        ))
+        mine_ref[:, cols] = (
+            acc_out[:, cols]
+            + jnp.dot(conv_s[...], co_all[:, cols], preferred_element_type=jnp.float32)
+        ).astype(jnp.bfloat16)
+        outs[i].start()
+
+    for group in direct + far_copies + over_sp:
+        for copy in group:
+            copy.wait_send()
+    for copy in [query_copy, memory_copy, stat_copy]:
+        copy.wait_send()
+    for k in range(1, n_sp):
+        @pl.when(s + k < n_sp)
+        def _(k=k):
+            for copy in sends[k - 1]:
+                copy.wait_send()
+
+        @pl.when(s >= k)
+        def _(k=k):
+            forwards[k - 1].wait_send()
+
+    @pl.when(s < n_sp - 1)
+    def _():
+        rim_copy.wait_send()
+
+    for copy in outs:
+        copy.wait()
+
+
+def fused_call(
+    sizes, x, mix_gain, rope_weight, taps, channel_gain, channel_shift,
+    latent_gain, memory_gain, query_gain, key_gain,
+    qd, md, cv, cg, qu, ku, vu, ho, co,
+):
+    n_fs, n_sp, n_tp = sizes
+    rows, model = x.shape
+    bf16, f32 = jnp.bfloat16, jnp.float32
+    vmem = pl.BlockSpec(memory_space=pltpu.VMEM)
+    hbm = pl.BlockSpec(memory_space=pl.ANY)
+    cosine, sine = table_rows(n_sp * rows)
+
+    def whole(w, dim=0):
+        return (w.shape[0] * n_fs, w.shape[1]) if dim == 0 else (w.shape[0], w.shape[1] * n_fs)
+
+    def scratch(*shape, dtype=f32):
+        return pltpu.VMEM(shape, dtype)
+
+    dma = pltpu.SemaphoreType.DMA
+    channels, lat = cv.shape[1], md.shape[1] * n_tp
+    rope = rope_weight.shape[1]
+    others = n_sp - 1
+    return pl.pallas_call(
+        functools.partial(fused_kernel, sizes),
+        out_shape=[jax.ShapeDtypeStruct((rows, ho.shape[1] * n_fs), bf16)] * 2,
+        in_specs=[vmem] * 12 + [hbm] * 9,
+        out_specs=[vmem] * 2,
+        scratch_shapes=[
+            scratch(*whole(md), dtype=bf16), scratch(*whole(qd), dtype=bf16),
+            scratch(*whole(ku), dtype=bf16), scratch(*whole(vu), dtype=bf16),
+            scratch(*whole(qu), dtype=bf16), scratch(*whole(cv), dtype=bf16),
+            scratch(*whole(cg), dtype=bf16), scratch(*whole(ho, 1), dtype=bf16),
+            scratch(*whole(co, 1), dtype=bf16),
+            scratch(rows, model, dtype=bf16), scratch(n_tp, rows, qd.shape[1], dtype=bf16),
+            scratch(n_tp, rows, md.shape[1], dtype=bf16),
+            scratch(n_sp, lat, rows, dtype=bf16), scratch(n_sp, rope, rows, dtype=bf16),
+            scratch(qu.shape[0] * n_fs, rows, dtype=bf16), scratch(qu.shape[1], rows),
+            scratch(n_sp, ku.shape[1], rows), scratch(n_sp, vu.shape[1], rows, dtype=bf16),
+            scratch(n_sp, rope, rows), scratch(n_sp, 1, rows),
+            scratch(n_sp, rows, rows), scratch(n_sp, rows, rows),
+            scratch(vu.shape[1], rows), scratch(rows, channels, dtype=bf16),
+            scratch(rows, channels), scratch(rows, channels),
+            scratch(rows, ho.shape[1] * n_fs),
+            scratch(rows + RIM, channels), scratch(RIM, channels, dtype=bf16),
+            scratch(RIM, channels, dtype=bf16), scratch(rows, channels),
+            scratch(2 * rows, 128), scratch(2 * rows, 128),
+            dma((9, 2)), dma((9, 2)), dma((9, 2)), dma((9, 2)),
+            dma((9, 3)), dma((9, 3)), dma((9,)), dma((2,)),
+            dma((others,)), dma((others,)), dma((others,)), dma((others,)),
+            dma((others,)), dma((others,)), dma((3,)), dma((3,)), dma((n_fs,)), dma((n_fs,)),
+        ],
+        compiler_params=pltpu.CompilerParams(
+            collective_id=1, has_side_effects=True, vmem_limit_bytes=60 * 1024 * 1024
+        ),
+    )(
+        x, mix_gain[None, :], rope_weight.T, taps, channel_gain[None, :], channel_shift[None, :],
+        latent_gain[None, :], memory_gain[None, :], query_gain[:, None], key_gain[:, None],
+        jnp.asarray(cosine), jnp.asarray(sine),
+        md, qd, ku, vu, qu, cv, cg, ho, co,
+    )
+
+
+def fused_local(
+    tokens, mix_gain, query_down, memory_down, rope_weight, query_up, key_up, value_up,
+    latent_gain, memory_gain, query_gain, key_gain, conv_value, conv_gate, conv_kernel,
+    channel_gain, channel_shift, heads_out, conv_out,
+):
+    mine, other = fused_call(
+        (lax.axis_size("fs"), lax.axis_size("sp"), lax.axis_size("tp")),
+        tokens[0], mix_gain, rope_weight, conv_kernel, channel_gain, channel_shift,
+        latent_gain, memory_gain, query_gain, key_gain,
+        query_down, memory_down, conv_value, conv_gate,
+        query_up, key_up, value_up, heads_out, conv_out,
+    )
+    return (mine.astype(jnp.float32) + other.astype(jnp.float32)).astype(jnp.bfloat16)[None]
+
+
 def solution(mesh):
     in_specs = (
         P("fs", "sp", None),
@@ -572,4 +1106,7 @@
         P("tp", "fs"),
     )
     out_specs = P("fs", "sp", None)
-    return jax.shard_map(local, mesh=mesh, in_specs=in_specs, out_specs=out_specs, check_vma=False)
+    n_fs, n_sp, n_tp = (mesh.shape[axis] for axis in ("fs", "sp", "tp"))
+    fits = n_fs == 4 and n_tp == 2 and n_sp in (2, 4)
+    body = fused_local if fits else local
+    return jax.shard_map(body, mesh=mesh, in_specs=in_specs, out_specs=out_specs, check_vma=False)

time: 126 us -> 114 us (0.905); the launches traced: 125 us -> 112 us
  matrix products: 9.17 us -> 0 us
  other arithmetic: 6.13 us -> 2.91 us
  waiting for transfers between devices: 2.65 us -> 0 us
  Pallas kernels: 103 us -> 105 us
    dot_general x6 -> x0, matrix products: 9.17 us -> none  [the longest x1 2.84 us: local(): jnp.dot(mixer_rows, out_weight, preferred_element_type=jnp.float32)]
    broadcast_in_dim x1 -> x3, local copies, waits for them, and re-layouts: 0.11 us -> 4.02 us  [the longest x1 1.37 us: fused_call(): query_gain[:, None]]
    reduce_sum x5 -> x0, other arithmetic: 3.11 us -> none  [the longest x1 2.2 us: attend(): row_total = row_total * factor + jnp.sum(weights, axis=2)]
    ppermute x1 -> x0, waiting for transfers between devices: 2.65 us -> none  [sum_groups(): other = lax.ppermute(partial, 'tp', [(0, 1), (1, 0)])]
    unnamed x23 -> x0, local copies, waits for them, and re-layouts: 2.05 us -> none
    pallas_call x1, Pallas kernels: 103 us -> 105 us  [fused_call(): pl.pallas_call(functools.partial(fused_kernel, sizes), out_shape=[jax.Sha...]
    broadcast_in_dim x1, other arithmetic: 1.36 us -> 2.91 us  [fused_local(): (mine.astype(jnp.float32) + other.astype(jnp.float32)).astype(jnp.bfloat16)]
    another operation x2 -> x0, local copies, waits for them, and re-layouts: 1.44 us -> none  [the longest x1 1.4 us: local(): whole_memory = jnp.concatenate(list(memory_parts), axis=1)]
  transfers between devices with their start and end apart: 1 -> 0, of which waited for: 1 -> 0; matrix products, arithmetic and copies ran while one was open for 0% -> 0% of each run, Pallas kernels for 0% -> 0%
where the time goes in v1:
time: 114 us; the launch traced here: 112 us
  Pallas kernels  105 us (92%)
  local copies, waits for them, and re-layouts  4.02 us (4%)
  other arithmetic  2.91 us (3%)
    pallas_call x1, Pallas kernels, fused_call(): pl.pallas_call(functools.partial(fused_kernel, sizes), out_shape=[jax.Sha...  105 us
    broadcast_in_dim x1, other arithmetic, fused_local(): (mine.astype(jnp.float32) + other.astype(jnp.float32)).astype(jnp.bfloat16)  2.91 us

profile of v1, /device:TPU:0, one launch (start us, length us, event | category | flops | bytes accessed | tf_op | source)
XLA Modules:
  0.0 111.7 jit_solution(7171504084957004063)
XLA Ops:
  0.0 1.3 %broadcast_in_dim.27.lgain_ref = f32[1,768]{1,0:T(1,128)} reshape(f32[768]{0:T(1024)} %param.29) | data formatting | bytes 6144 | tf_op jit(solution)/shard_map/broadcast_in_dim | solution.py:1065
  1.3 1.4 %copy.22.qgain_ref = f32[96,1]{1,0:T(8,128)} copy(f32[96,1]{0,1:T(1,128)} %bitcast.16) | data formatting | bytes 768 | tf_op jit(solution)/shard_map/broadcast_in_dim | solution.py:1065
  2.7 1.4 %copy.23.kgain_ref = f32[96,1]{1,0:T(8,128)} copy(f32[96,1]{0,1:T(1,128)} %bitcast.17) | data formatting | bytes 768 | tf_op jit(solution)/shard_map/broadcast_in_dim | solution.py:1065
  4.0 104.8 %shard_map.199 = (bf16[256,2048]{1,0:T(8,128)(2,1)}, bf16[256,2048]{1,0:T(8,128)(2,1)}) custom-call(bf16[256,2048]{1,0:T(8,128)(2,1)} %bitcast.10, f32[1,2048]{1,0:T(1,128)} %bitcast.12, bf16[32,2048]{1,0:T(8,128)(2,1)} %bitcast.11, bf16[31,512]{1,0:T(8,128)(2,1)} %taps_ref.1, f32[1,512]{1,0:T(1,128)} %bitcast.13, f32[1,512]{1,0:T(1,128)} %bitcast.14, ...), custom_call_target="tpu_custom_call" | custom-call | tf_op jit(solution)/shard_map/pallas_call | solution.py:1031
  108.8 2.9 %fusion = bf16[1,256,2048]{2,1,0:T(8,128)(2,1)} fusion(bf16[256,2048]{1,0:T(8,128)(2,1)} %get-tuple-element.8, bf16[256,2048]{1,0:T(8,128)(2,1)} %get-tuple-element.7), kind=kLoop, calls=%fused_computation.1 | loop fusion | flops 2097152 | bytes 3145728 | tf_op jit(solution)/shard_map/broadcast_in_dim | solution.py:1083

commit v2 on v1

--- a/solution.py
+++ b/solution.py
@@ -565,25 +565,36 @@
     )
 
 
+def swapped_rows(count, eighths):
+    return (count * eighths // 8) // 16 * 16
+
+
 def fused_kernel(
     sizes,
-    x_ref, gain_ref, rope_ref, taps_ref, cgain_ref, cshift_ref,
+    x_hbm, gain_hbm, rope_hbm, taps_hbm, cgain_hbm, cshift_hbm,
+    lgain_hbm, mgain_hbm, qgain_hbm, kgain_hbm, cos_hbm, sin_hbm,
+    qd, md, ku, vu, qu, cv, cg, ho, co,
+    out_hbm,
+    gain_ref, rope_ref, taps_ref, cgain_ref, cshift_ref,
     lgain_ref, mgain_ref, qgain_ref, kgain_ref, cos_ref, sin_ref,
-    md, qd, ku, vu, qu, cv, cg, ho, co,
-    mine_ref, other_ref,
-    md_all, qd_all, ku_all, vu_all, qu_all, cv_all, cg_all, ho_all, co_all,
-    normed, lq_all, lm_all, mem_all, rr_all, qn_t, q_t, k_t, v_t, turned, ropesq, bias, scores,
-    att_t, conv_s, acc_v, acc_g, acc_out, ext, tail, rim, sums, stats, stats_all,
-    send_d, recv_d, send_r, recv_r, send_z, recv_z, local_sem, rim_sem,
-    sp_send, sp_recv, rr_send, rr_recv, fw_send, fw_recv, tp_send, tp_recv, out_send, out_recv,
+    qd_all, md_all, ku_all, vu_all, qu_all, cv_all, cg_all, ho_all, co_all,
+    x_all, normed, lq_all, lq_out, lm_all, mem_all, rr_all, qn_t, q_t, k_t, v_t,
+    turned, ropesq, qcol, kcol, bias, scores,
+    att_t, conv_s, acc_v, acc_g, acc_out, gate_out, gate_in, ext, tail, rim, sums, stats, stats_all,
+    mine_ref, other_ref, whole_ref,
+    send_d, recv_d, send_r, recv_r, send_z, recv_z, local_sem, small_sem, rim_sem, x_sem,
+    part_sem, sp_send, sp_recv, fw_send, fw_recv, tp_send, tp_recv, out_send, out_recv, store_sem,
 ):
     n_fs, n_sp, n_tp = sizes
     f = lax.axis_index("fs")
     s = lax.axis_index("sp")
     t = lax.axis_index("tp")
     parity = lax.rem(s, 2)
-    partner = s + 1 - 2 * parity
+    couple = lax.div(s, 2)
+    couples = n_sp // 2
+    partner = {"sp": s + 1 - 2 * parity}
     twin = {"tp": 1 - t}
+    even, odd = parity == 0, parity == 1
 
     barrier = pltpu.get_barrier_semaphore()
     for axis, at, count in (("fs", f, n_fs), ("sp", s, n_sp), ("tp", t, n_tp)):
@@ -591,135 +602,191 @@
             pl.semaphore_signal(
                 barrier, inc=1, device_id={axis: lax.rem(at + k, count)}, device_id_type=MESH_ID
             )
-    pl.semaphore_wait(barrier, n_fs + n_sp + n_tp - 3)
-
-    jobs = [
-        (md, md_all, 0), (qd, qd_all, 0), (ku, ku_all, 0), (vu, vu_all, 0), (qu, qu_all, 0),
-        (cv, cv_all, 0), (cg, cg_all, 0), (ho, ho_all, 1), (co, co_all, 1),
+
+    rows = x_hbm.shape[0]
+    x_own = pltpu.make_async_copy(x_hbm, x_all.at[parity], x_sem.at[0])
+    x_own.start()
+    small = [
+        pltpu.make_async_copy(source, landing, small_sem.at[i])
+        for i, (source, landing) in enumerate((
+            (gain_hbm, gain_ref), (rope_hbm, rope_ref), (taps_hbm, taps_ref),
+            (cgain_hbm, cgain_ref), (cshift_hbm, cshift_ref), (lgain_hbm, lgain_ref),
+            (mgain_hbm, mgain_ref), (qgain_hbm, qgain_ref), (kgain_hbm, kgain_ref),
+            (cos_hbm, cos_ref), (sin_hbm, sin_ref),
+        ))
     ]
-    last = len(jobs) - 1
-    ahead = 4
-
-    def place(whole, shard, dim, owner, start, count):
-        rows, cols = shard.shape
-        if dim == 0:
-            return whole.at[pl.ds(pl.multiple_of(owner * rows + start, 16), count), :]
-        return whole.at[
-            pl.ds(pl.multiple_of(start, 16), count),
-            pl.ds(pl.multiple_of(owner * cols, 128), cols),
-        ]
+    for copy in small:
+        copy.start()
+
+    def remote(source, landing, send, recv, device):
+        return pltpu.make_async_remote_copy(
+            src_ref=source, dst_ref=landing, send_sem=send, recv_sem=recv,
+            device_id=device, device_id_type=MESH_ID,
+        )
+
+    share = rows // n_tp
+    slab = pl.ds(pl.multiple_of(t * share, 16), share)
+    x_send = remote(
+        x_hbm.at[slab, :], x_all.at[parity, slab, :], x_sem.at[1], x_sem.at[2], partner
+    )
+    theirs = x_all.at[1 - parity, slab, :]
+    x_forward = remote(theirs, theirs, x_sem.at[3], x_sem.at[4], twin)
 
     near_x = f + 1 - 2 * lax.rem(f, 2)
     near_y = lax.rem(f + 2, 4)
     far = lax.rem(near_x + 2, 4)
     sources = [near_x, near_y]
 
-    direct, far_copies, over_sp, own = [], [], [], []
-    for a, (shard, whole, dim) in enumerate(jobs):
-        rows = shard.shape[0]
-        less = 0 if a == last else relayed_rows(rows, True)
-        start = parity * less
-        count = rows - less
-        direct.append([
-            pltpu.make_async_remote_copy(
-                src_ref=shard.at[pl.ds(pl.multiple_of(start, 16), count), :],
-                dst_ref=place(whole, shard, dim, f, start, count),
-                send_sem=send_d.at[a, k], recv_sem=recv_d.at[a, k],
-                device_id={"fs": target}, device_id_type=MESH_ID,
+    def job(a, shard, whole, swap, dim=0, first=0, count=None):
+        depth, cols = shard.shape
+        count = depth if count is None else count
+        less = swapped_rows(count, swap)
+        kept = count - less
+
+        def place(owner, start, size):
+            if dim == 0:
+                return whole.at[pl.ds(pl.multiple_of(owner * depth + start, 16), size), :]
+            return whole.at[
+                pl.ds(pl.multiple_of(start, 16), size),
+                pl.ds(pl.multiple_of(owner * cols, 128), cols),
+            ]
+
+        start = first + parity * less
+        direct = [
+            remote(
+                shard.at[pl.ds(pl.multiple_of(start, 16), kept), :], place(f, start, kept),
+                send_d.at[a, k], recv_d.at[a, k], {"fs": target},
             )
             for k, target in enumerate(sources)
-        ])
-        halves = []
-        half = (count // 2 + 15) // 16 * 16
+        ]
+        half = (kept // 2 + 15) // 16 * 16
+        relays = []
         for k, (owner, target, begin, size) in enumerate((
-            (near_y, near_x, start, half), (near_x, near_y, start + half, count - half)
+            (near_y, near_x, start, half), (near_x, near_y, start + half, kept - half)
         )):
-            piece = place(whole, shard, dim, owner, begin, size)
-            halves.append(pltpu.make_async_remote_copy(
-                src_ref=piece, dst_ref=piece,
-                send_sem=send_r.at[a, k], recv_sem=recv_r.at[a, k],
-                device_id={"fs": target}, device_id_type=MESH_ID,
-            ))
-        far_copies.append(halves)
+            piece = place(owner, begin, size)
+            relays.append(remote(piece, piece, send_r.at[a, k], recv_r.at[a, k], {"fs": target}))
         across = []
         if less:
-            lack = parity * (rows - less)
             for k, owner in enumerate(sources + [far]):
-                piece = place(whole, shard, dim, owner, lack, less)
-                across.append(pltpu.make_async_remote_copy(
-                    src_ref=piece, dst_ref=piece,
-                    send_sem=send_z.at[a, k], recv_sem=recv_z.at[a, k],
-                    device_id={"sp": partner}, device_id_type=MESH_ID,
-                ))
-        over_sp.append(across)
-        own.append(pltpu.make_async_copy(
-            shard, place(whole, shard, dim, f, 0, rows), local_sem.at[a]
-        ))
+                piece = place(owner, first + parity * kept, less)
+                across.append(remote(piece, piece, send_z.at[a, k], recv_z.at[a, k], partner))
+        own = pltpu.make_async_copy(
+            shard.at[pl.ds(first, count), :], place(f, first, count), local_sem.at[a]
+        )
+        return direct, relays, across, own
+
+    wide = cv.shape[1] // 2
+    side = pl.ds(pl.multiple_of(parity * wide, 128), wide)
+    half_rows = ho.shape[0] // 2
+    plan = [
+        [(even, qd, qd_all, 0), (odd, md, md_all, 0)],
+        [(None, ku, ku_all, 4)], [(None, vu, vu_all, 4)], [(None, qu, qu_all, 4)],
+        [(None, cv.at[:, side], cv_all, 0)], [(None, cg.at[:, side], cg_all, 0)],
+        [(None, ho, ho_all, 4, 1, 0, half_rows)], [(None, ho, ho_all, 4, 1, half_rows, half_rows)],
+        [(None, co, co_all, 3, 1, 0, half_rows)], [(None, co, co_all, 0, 1, half_rows, half_rows)],
+    ]
+    jobs = [[(who[0], job(a, *who[1:])) for who in group] for a, group in enumerate(plan)]
+    last = len(jobs) - 1
+    ahead = 3
+
+    def each(a, action):
+        for condition, parts in jobs[a]:
+            if condition is None:
+                action(parts)
+            else:
+                pl.when(condition)(functools.partial(action, parts))
 
     def begin_array(a):
+        def start(parts):
+            for copy in parts[0]:
+                copy.start()
+
         if a <= last:
-            for copy in direct[a]:
+            each(a, start)
+
+    def finish_far(a):
+        def go(parts):
+            with jax.named_scope(f"far_{a}"):
+                for copy in parts[1]:
+                    copy.wait_recv()
+            for copy in parts[2][len(sources):]:
                 copy.start()
 
-    def finish_far(a):
-        for copy in far_copies[a]:
-            copy.wait_recv()
-        for copy in over_sp[a][len(sources):]:
-            copy.start()
+        each(a, go)
 
     def tick(a):
-        for copy in direct[a]:
-            copy.wait_recv()
-        for copy in far_copies[a]:
-            copy.start()
+        def go(parts):
+            with jax.named_scope(f"direct_{a}"):
+                for copy in parts[0]:
+                    copy.wait_recv()
+            for copy in parts[1]:
+                copy.start()
+
+        def swap(parts):
+            for copy in parts[2][: len(sources)]:
+                copy.start()
+
+        each(a, go)
         begin_array(a + ahead)
-        for copy in over_sp[a][: len(sources)]:
-            copy.start()
-        if a >= 1:
-            finish_far(a - 1)
+        each(a, swap)
 
     def complete(a):
-        own[a].wait()
-        for copy in over_sp[a]:
-            copy.wait_recv()
-
+        def go(parts):
+            with jax.named_scope(f"across_{a}"):
+                parts[3].wait()
+                for copy in parts[2]:
+                    copy.wait_recv()
+
+        each(a, go)
+
+    with jax.named_scope("entry"):
+        pl.semaphore_wait(barrier, n_fs + n_sp + n_tp - 3)
+    x_send.start()
     for a in range(ahead):
         begin_array(a)
-    for copy in own:
-        copy.start()
-
-    rows = x_ref.shape[0]
+    for a in range(last + 1):
+        each(a, lambda parts: parts[3].start())
+    with jax.named_scope("small_wait"):
+        for copy in small:
+            copy.wait()
+        x_own.wait()
+
     part = 32
 
-    @pl.loop(0, rows // part)
-    def _(i):
-        at = pl.ds(pl.multiple_of(i * part, part), part)
-        x = x_ref[at, :].astype(jnp.float32)
-        scale = lax.rsqrt(jnp.mean(x * x, axis=-1, keepdims=True) + epsilon)
-        normed[at, :] = (x * scale * gain_ref[...]).astype(jnp.bfloat16)
-
-    depth = qd.shape[0]
-
-    def project(weight, acc):
-        acc[...] = jnp.zeros_like(acc)
-
-        @pl.loop(0, n_fs)
+    def norm_block(b):
+        @pl.loop(0, rows // part)
         def _(i):
-            at = pl.ds(pl.multiple_of(i * depth, depth), depth)
-            acc[...] += jnp.dot(
-                normed[:, at], weight[at, :], preferred_element_type=jnp.float32
-            )
-
-    rr_all[s] = lax.dot_general(
-        rope_ref[...], normed[...], (((1,), (1,)), ((), ())), preferred_element_type=jnp.float32
-    ).astype(jnp.bfloat16)
-
+            at = pl.ds(pl.multiple_of(i * part, part), part)
+            x = x_all[b, at, :].astype(jnp.float32)
+            scale = lax.rsqrt(jnp.mean(x * x, axis=-1, keepdims=True) + epsilon)
+            normed[b, at, :] = (x * scale * gain_ref[...]).astype(jnp.bfloat16)
+
+        rr_all[2 * couple + b] = lax.dot_general(
+            rope_ref[...], normed[b], (((1,), (1,)), ((), ())), preferred_element_type=jnp.float32
+        ).astype(jnp.bfloat16)
+
+    norm_block(parity)
     half_rope = QK_ROPE // 2
 
-    @pl.loop(s + 1, n_sp)
+    def column(row_ref, col_ref):
+        shape = (QK_DIM, QK_DIM)
+        here = lax.broadcasted_iota(jnp.int32, shape, 0) == lax.broadcasted_iota(jnp.int32, shape, 1)
+        spread_row = jnp.broadcast_to(row_ref[...], shape)
+        picked = jnp.sum(jnp.where(here, spread_row, 0.0), axis=1, keepdims=True)
+        col_ref[...] = jnp.broadcast_to(picked, col_ref.shape)
+
+    column(qgain_ref, qcol)
+    column(kgain_ref, kcol)
+
+    @pl.loop(2 * couple + 2, n_sp)
     def _(j):
         mem_all[j] = jnp.zeros(mem_all.shape[1:], jnp.bfloat16)
         rr_all[j] = jnp.zeros(rr_all.shape[1:], jnp.bfloat16)
+
+    @pl.when(even)
+    def _():
+        mem_all[s + 1] = jnp.zeros(mem_all.shape[1:], jnp.bfloat16)
 
     @pl.loop(0, n_sp)
     def _(j):
@@ -729,100 +796,162 @@
             lax.div(key_at, SEG) <= lax.div(query_at, SEG), 0.0, masked_score
         )
 
-    def to_twin(kind, source, landing):
-        return pltpu.make_async_remote_copy(
-            src_ref=source, dst_ref=landing,
-            send_sem=tp_send.at[kind], recv_sem=tp_recv.at[kind],
-            device_id=twin, device_id_type=MESH_ID,
-        )
-
-    query_copy = to_twin(0, lq_all.at[t], lq_all.at[t])
-    memory_copy = to_twin(1, lm_all.at[t], lm_all.at[t])
-    stat_copy = to_twin(2, stats, stats_all)
+    tick(0)
+    with jax.named_scope("x_wait"):
+        x_send.wait_recv()
+    x_forward.start()
+    tick(1)
+    with jax.named_scope("x_forward"):
+        x_forward.wait_recv()
+    norm_block(1 - parity)
+    tick(2)
+    finish_far(0)
+
+    depth = qd.shape[0]
+
+    def project(weight, b, acc):
+        acc[...] = jnp.zeros_like(acc)
+
+        @pl.loop(0, n_fs)
+        def _(i):
+            at = pl.ds(pl.multiple_of(i * depth, depth), depth)
+            acc[...] += jnp.dot(
+                normed[b, :, at], weight[at, :], preferred_element_type=jnp.float32
+            )
 
     lat = md.shape[1]
+    lat_q = qd.shape[1]
     held = pl.ds(pl.multiple_of(t * lat, lat), lat)
-    sends, forwards = [], []
-    for k in range(1, n_sp):
-        peer = {"sp": lax.rem(s + k, n_sp)}
-        sends.append([
-            pltpu.make_async_remote_copy(
-                src_ref=mem_all.at[s, held, :], dst_ref=mem_all.at[s, held, :],
-                send_sem=sp_send.at[k - 1], recv_sem=sp_recv.at[k - 1],
-                device_id=peer, device_id_type=MESH_ID,
-            ),
-            pltpu.make_async_remote_copy(
-                src_ref=rr_all.at[s], dst_ref=rr_all.at[s],
-                send_sem=rr_send.at[k - 1], recv_sem=rr_recv.at[k - 1],
-                device_id=peer, device_id_type=MESH_ID,
-            ),
-        ])
-        behind = mem_all.at[lax.rem(s + n_sp - k, n_sp), held, :]
-        forwards.append(pltpu.make_async_remote_copy(
-            src_ref=behind, dst_ref=behind,
-            send_sem=fw_send.at[k - 1], recv_sem=fw_recv.at[k - 1],
-            device_id=twin, device_id_type=MESH_ID,
-        ))
-
-    tick(0)
-    tick(1)
-    tick(2)
+    query_across = remote(lq_out, lq_all.at[t], part_sem.at[0], part_sem.at[1], partner)
+    query_copy = remote(lq_all.at[t], lq_all.at[t], tp_send.at[0], tp_recv.at[0], twin)
+    memory_copy = remote(lm_all.at[t], lm_all.at[t], tp_send.at[1], tp_recv.at[1], twin)
+    stat_copy = remote(stats, stats_all, tp_send.at[2], tp_recv.at[2], twin)
+    gate_across = remote(gate_out, gate_in, part_sem.at[2], part_sem.at[3], partner)
+
     complete(0)
-    project(md_all, acc_v.at[:, pl.ds(0, lat)])
-    lm_all[t, :, :] = acc_v[:, :lat].astype(jnp.bfloat16)
-    memory_copy.start()
+
+    @pl.when(even)
+    def _():
+        project(qd_all, 1, acc_out.at[:, pl.ds(0, lat_q)])
+        lq_out[...] = acc_out[:, :lat_q].astype(jnp.bfloat16)
+        query_across.start()
+        project(qd_all, 0, acc_out.at[:, pl.ds(0, lat_q)])
+        lq_all[t] = acc_out[:, :lat_q].astype(jnp.bfloat16)
+        query_copy.start()
+
+    @pl.when(odd)
+    def _():
+        for b in range(2):
+            project(md_all, b, acc_v.at[:, pl.ds(0, lat)])
+            lm_all[t, b] = acc_v[:, :lat].astype(jnp.bfloat16)
+        memory_copy.start()
+
     tick(3)
-    complete(1)
-    wide = qd.shape[1]
-    project(qd_all, acc_g.at[:, pl.ds(0, wide)])
-    lq_all[t, :, :] = acc_g[:, :wide].astype(jnp.bfloat16)
-    query_copy.start()
-
-    def normed_columns(parts, gains, put):
-        width = parts.shape[2]
-
+
+    def normed_columns(parts, width, gain_at, put):
         @pl.loop(0, rows // 128)
         def _(i):
             at = pl.ds(pl.multiple_of(i * 128, 128), 128)
-            pieces = [parts[g, at, :].astype(jnp.float32) for g in range(n_tp)]
+            pieces = [parts(g, at).astype(jnp.float32) for g in range(n_tp)]
             total = sum(jnp.sum(p * p, axis=-1, keepdims=True) for p in pieces)
             scale = lax.rsqrt(total / (width * n_tp) + epsilon)
             for g in range(n_tp):
-                gain = gains[:, g * width : (g + 1) * width]
-                shaped = (pieces[g] * scale * gain).astype(jnp.bfloat16)
+                shaped = (pieces[g] * scale * gain_at(g * width, width)).astype(jnp.bfloat16)
                 put(g * width, width, at, shaped.astype(jnp.float32).T.astype(jnp.bfloat16))
 
-    def put_memory(begin, width, at, piece):
-        mem_all[s, begin : begin + width, at] = piece
+    mine_block = mem_all.at[s, held, :]
+    back = remote(
+        mem_all.at[2 * couple, held, :], mem_all.at[2 * couple, held, :],
+        part_sem.at[4], part_sem.at[5], partner,
+    )
+    back_forward = remote(mine_block, mine_block, fw_send.at[couples - 1], fw_recv.at[couples - 1], twin)
+    pair = pl.ds(2 * couple, 2)
+    onward, forwards = [], []
+    for d in range(1, couples):
+        group = []
+        later = lax.rem(couple + d, couples)
+        for e in range(2):
+            target = {"sp": 2 * later + e}
+            group.append((
+                remote(
+                    mem_all.at[pair, held, :], mem_all.at[pair, held, :],
+                    sp_send.at[d - 1, e, 0], sp_recv.at[d - 1, 0], target,
+                ),
+                remote(
+                    rr_all.at[pair], rr_all.at[pair],
+                    sp_send.at[d - 1, e, 1], sp_recv.at[d - 1, 1], target,
+                ),
+            ))
+        onward.append(group)
+        earlier = mem_all.at[pl.ds(2 * lax.rem(couple + couples - d, couples), 2), held, :]
+        forwards.append(remote(earlier, earlier, fw_send.at[d - 1], fw_recv.at[d - 1], twin))
+
+    @pl.when(odd)
+    def _():
+        with jax.named_scope("memory_wait"):
+            memory_copy.wait_recv()
+        for b in (1, 0):
+            def put_memory(begin, width, at, piece, b=b):
+                mem_all[2 * couple + b, begin : begin + width, at] = piece
+
+            normed_columns(
+                lambda g, at, b=b: lm_all[g, b, at, :], lat,
+                lambda begin, width: mgain_ref[:, begin : begin + width], put_memory,
+            )
+        for d in range(1, couples):
+            @pl.when(couple + d < couples)
+            def _(d=d):
+                for e in range(2):
+                    for copy in onward[d - 1][e]:
+                        copy.start()
+        back.start()
+        with jax.named_scope("query_across"):
+            query_across.wait_recv()
+        query_copy.start()
+
+    finish_far(1)
+    tick(4)
 
     def put_query(begin, width, at, piece):
         qn_t[begin : begin + width, at] = piece
 
-    memory_copy.wait_recv()
-    normed_columns(lm_all, mgain_ref, put_memory)
-    for k in range(1, n_sp):
-        @pl.when(s + k < n_sp)
-        def _(k=k):
-            for copy in sends[k - 1]:
-                copy.start()
-
-    tick(4)
-    query_copy.wait_recv()
-    normed_columns(lq_all, lgain_ref, put_query)
+    with jax.named_scope("query_wait"):
+        query_copy.wait_recv()
+    normed_columns(
+        lambda g, at: lq_all[g, at, :], lat_q,
+        lambda begin, width: jnp.concatenate(
+            [lgain_ref[r : r + 1, :] for r in range(begin // 128, (begin + width) // 128)], axis=1
+        ),
+        put_query,
+    )
+    finish_far(2)
+
+    @pl.when(even)
+    def _():
+        with jax.named_scope("back_wait"):
+            back.wait_recv()
+        back_forward.start()
+
+    for d in range(1, couples):
+        @pl.when(couple >= d)
+        def _(d=d):
+            with jax.named_scope(f"behind_{d}"):
+                for copy in onward[d - 1][0]:
+                    copy.wait_recv()
+            forwards[d - 1].start()
+    complete(1)
     complete(2)
-    tick(5)
-    complete(3)
-
-    for k in range(1, n_sp):
-        @pl.when(s >= k)
-        def _(k=k):
-            for copy in sends[k - 1]:
-                copy.wait_recv()
-            forwards[k - 1].start()
-    for k in range(1, n_sp):
-        @pl.when(s >= k)
-        def _(k=k):
-            forwards[k - 1].wait_recv()
+
+    @pl.when(even)
+    def _():
+        with jax.named_scope("back_forward"):
+            back_forward.wait_recv()
+
+    for d in range(1, couples):
+        @pl.when(couple >= d)
+        def _(d=d):
+            with jax.named_scope(f"forward_{d}"):
+                forwards[d - 1].wait_recv()
 
     @pl.loop(0, n_sp)
     def _(j):
@@ -830,16 +959,18 @@
         v_t[j] = dot_heads(vu_all[...], mem_all[j]).astype(jnp.bfloat16)
         shared = rr_all[j].astype(jnp.float32)
         ropesq[j] = jnp.sum(shared * shared, axis=0, keepdims=True)
-        shared = shared * kgain_ref[QK_NOPE:, :]
-        front, back = shared[:half_rope], shared[half_rope:]
+        shared = shared * kcol[QK_NOPE:, :]
+        front, back_half = shared[:half_rope], shared[half_rope:]
         at = pl.ds(pl.multiple_of(j * rows, rows), rows)
         cosine, sine = cos_ref[:, at], sin_ref[:, at]
         turned[j] = jnp.concatenate(
-            [front * cosine - back * sine, front * sine + back * cosine], axis=0
+            [front * cosine - back_half * sine, front * sine + back_half * cosine], axis=0
         )
 
+    tick(5)
+    finish_far(3)
     tick(6)
-    complete(4)
+    complete(3)
     q_t[...] = dot_heads(qu_all[...], qn_t[...])
     heads = qu.shape[1] // QK_DIM
     here = pl.ds(pl.multiple_of(s * rows, rows), rows)
@@ -847,11 +978,16 @@
 
     def head(h):
         q = q_t[pl.ds(pl.multiple_of(h * QK_DIM, QK_DIM), QK_DIM), :]
-        q = q * lax.rsqrt(jnp.mean(q * q, axis=0, keepdims=True) + epsilon) * qgain_ref[...]
-        front, back = q[QK_NOPE : QK_NOPE + half_rope], q[QK_NOPE + half_rope :]
+        q = q * lax.rsqrt(jnp.mean(q * q, axis=0, keepdims=True) + epsilon) * qcol[...]
+        front, back_half = q[QK_NOPE : QK_NOPE + half_rope], q[QK_NOPE + half_rope :]
         cosine, sine = cos_ref[:, here], sin_ref[:, here]
         q = jnp.concatenate(
-            [q[:QK_NOPE], front * cosine - back * sine, front * sine + back * cosine], axis=0
+            [
+                q[:QK_NOPE],
+                front * cosine - back_half * sine,
+                front * sine + back_half * cosine,
+            ],
+            axis=0,
         ).astype(jnp.bfloat16)
         krow = pl.ds(pl.multiple_of(h * QK_NOPE, QK_NOPE), QK_NOPE)
         vrow = pl.ds(pl.multiple_of(h * V_DIM, V_DIM), V_DIM)
@@ -862,7 +998,7 @@
                 (jnp.sum(nope * nope, axis=0, keepdims=True) + ropesq[j]) / QK_DIM + epsilon
             )
             key = jnp.concatenate(
-                [nope * scale * kgain_ref[:QK_NOPE, :], turned[j] * scale], axis=0
+                [nope * scale * kcol[:QK_NOPE, :], turned[j] * scale], axis=0
             ).astype(jnp.bfloat16)
             block = dot_heads(key, q) + bias[j]
             scores[j] = block
@@ -879,24 +1015,33 @@
         att_t[vrow, :] = summed / total
 
     pl.loop(0, heads // 2)(head)
+    finish_far(4)
     tick(7)
     pl.loop(heads // 2, heads)(head)
+    finish_far(5)
+    complete(4)
     complete(5)
-    project(cv_all, acc_v)
-    tick(8)
-    complete(6)
-    project(cg_all, acc_g)
-
-    @pl.loop(0, rows // part)
-    def _(i):
-        at = pl.ds(pl.multiple_of(i * part, part), part)
-        gated = (acc_v[at, :] * jax.nn.sigmoid(acc_g[at, :])).astype(jnp.bfloat16)
-        ext[pl.ds(pl.multiple_of(RIM + i * part, part), part), :] = gated.astype(jnp.float32)
+    for other_block in (True, False):
+        b = 1 - parity if other_block else parity
+        project(cv_all, b, acc_v)
+        project(cg_all, b, acc_g)
+        gated = (acc_v[...] * jax.nn.sigmoid(acc_g[...])).astype(jnp.bfloat16)
+        if other_block:
+            gate_out[...] = gated
+            gate_across.start()
+            tick(8)
+            finish_far(6)
+        else:
+            ext[pl.ds(RIM, rows), side] = gated.astype(jnp.float32)
+    with jax.named_scope("gate_wait"):
+        gate_across.wait_recv()
+    ext[
+        pl.ds(RIM, rows), pl.ds(pl.multiple_of((1 - parity) * wide, 128), wide)
+    ] = gate_in[...].astype(jnp.float32)
 
     tail[...] = ext[pl.ds(rows, RIM), :].astype(jnp.bfloat16)
-    rim_copy = pltpu.make_async_remote_copy(
-        src_ref=tail, dst_ref=rim, send_sem=rim_sem.at[0], recv_sem=rim_sem.at[1],
-        device_id={"sp": lax.rem(s + 1, n_sp)}, device_id_type=MESH_ID,
+    rim_copy = remote(
+        tail, rim, rim_sem.at[0], rim_sem.at[1], {"sp": lax.rem(s + 1, n_sp)}
     )
 
     @pl.when(s < n_sp - 1)
@@ -905,7 +1050,8 @@
 
     @pl.when(s > 0)
     def _():
-        rim_copy.wait_recv()
+        with jax.named_scope("rim_wait"):
+            rim_copy.wait_recv()
         ext[pl.ds(0, RIM), :] = rim[...].astype(jnp.float32)
 
     @pl.when(s == 0)
@@ -927,8 +1073,10 @@
             sums[pl.ds(r, block), cols] = total
 
     tiles = ext.shape[1] // 128
-    pl.loop(0, tiles)(convolve)
-    finish_far(last)
+    pl.loop(0, tiles // 2)(convolve)
+    finish_far(7)
+    pl.loop(tiles // 2, tiles)(convolve)
+    tick(9)
 
     @pl.loop(0, rows // part)
     def _(i):
@@ -942,6 +1090,8 @@
         )
 
     stat_copy.start()
+    finish_far(8)
+    complete(6)
     complete(7)
     att = att_t[...].T.astype(jnp.bfloat16)
     span = ho.shape[1]
@@ -951,7 +1101,8 @@
         cols = pl.ds(pl.multiple_of(i * span, span), span)
         acc_out[:, cols] = jnp.dot(att, ho_all[:, cols], preferred_element_type=jnp.float32)
 
-    stat_copy.wait_recv()
+    with jax.named_scope("stat_wait"):
+        stat_copy.wait_recv()
     channels = ext.shape[1] * n_tp
 
     @pl.loop(0, rows // part)
@@ -968,42 +1119,83 @@
             shaped * cgain_ref[...] + cshift_ref[...]
         ).astype(jnp.bfloat16)
 
+    finish_far(last)
     complete(8)
+
+    @pl.loop(0, n_fs)
+    def _(i):
+        cols = pl.ds(pl.multiple_of(i * span, span), span)
+        acc_out[:, cols] += jnp.dot(
+            conv_s[:, :half_rows], co_all[:half_rows, cols], preferred_element_type=jnp.float32
+        )
+
+    complete(last)
     outs = []
     for i in range(n_fs):
         cols = slice(i * span, (i + 1) * span)
-        outs.append(pltpu.make_async_remote_copy(
-            src_ref=mine_ref.at[:, cols], dst_ref=other_ref.at[:, cols],
-            send_sem=out_send.at[i], recv_sem=out_recv.at[i],
-            device_id=twin, device_id_type=MESH_ID,
+        outs.append(remote(
+            mine_ref.at[:, cols], other_ref.at[:, cols], out_send.at[i], out_recv.at[i], twin
         ))
         mine_ref[:, cols] = (
             acc_out[:, cols]
-            + jnp.dot(conv_s[...], co_all[:, cols], preferred_element_type=jnp.float32)
+            + jnp.dot(
+                conv_s[:, half_rows:], co_all[half_rows:, cols],
+                preferred_element_type=jnp.float32,
+            )
         ).astype(jnp.bfloat16)
         outs[i].start()
 
-    for group in direct + far_copies + over_sp:
-        for copy in group:
+    def drain(parts):
+        for copy in parts[0] + parts[1] + parts[2]:
             copy.wait_send()
-    for copy in [query_copy, memory_copy, stat_copy]:
+
+    for a in range(last + 1):
+        each(a, drain)
+    for copy in (x_send, x_forward, query_copy, stat_copy, gate_across):
         copy.wait_send()
-    for k in range(1, n_sp):
-        @pl.when(s + k < n_sp)
-        def _(k=k):
-            for copy in sends[k - 1]:
-                copy.wait_send()
-
-        @pl.when(s >= k)
-        def _(k=k):
-            forwards[k - 1].wait_send()
+
+    @pl.when(even)
+    def _():
+        query_across.wait_send()
+        back_forward.wait_send()
+
+    @pl.when(odd)
+    def _():
+        memory_copy.wait_send()
+        back.wait_send()
+        for d in range(1, couples):
+            @pl.when(couple + d < couples)
+            def _(d=d):
+                for e in range(2):
+                    for copy in onward[d - 1][e]:
+                        copy.wait_send()
+
+    for d in range(1, couples):
+        @pl.when(couple >= d)
+        def _(d=d):
+            forwards[d - 1].wait_send()
 
     @pl.when(s < n_sp - 1)
     def _():
         rim_copy.wait_send()
 
-    for copy in outs:
-        copy.wait()
+    stores = []
+    for i in range(n_fs):
+        cols = slice(i * span, (i + 1) * span)
+        with jax.named_scope(f"out_wait_{i}"):
+            outs[i].wait_recv()
+        whole_ref[:, cols] = (
+            mine_ref[:, cols].astype(jnp.float32) + other_ref[:, cols].astype(jnp.float32)
+        ).astype(jnp.bfloat16)
+        stores.append(pltpu.make_async_copy(
+            whole_ref.at[:, cols], out_hbm.at[:, cols], store_sem.at[i]
+        ))
+        stores[i].start()
+    with jax.named_scope("store_wait"):
+        for copy in outs:
+            copy.wait_send()
+        for copy in stores:
+            copy.wait()
 
 
 def fused_call(
@@ -1014,12 +1206,17 @@
     n_fs, n_sp, n_tp = sizes
     rows, model = x.shape
     bf16, f32 = jnp.bfloat16, jnp.float32
-    vmem = pl.BlockSpec(memory_space=pltpu.VMEM)
     hbm = pl.BlockSpec(memory_space=pl.ANY)
     cosine, sine = table_rows(n_sp * rows)
-
-    def whole(w, dim=0):
-        return (w.shape[0] * n_fs, w.shape[1]) if dim == 0 else (w.shape[0], w.shape[1] * n_fs)
+    small = [
+        mix_gain[None, :], rope_weight.T, taps, channel_gain[None, :], channel_shift[None, :],
+        latent_gain.reshape(-1, 128), memory_gain[None, :], query_gain[None, :],
+        key_gain[None, :], jnp.asarray(cosine), jnp.asarray(sine),
+    ]
+
+    def whole(w, dim=0, parts=1):
+        rows_w, cols_w = w.shape[0], w.shape[1] // parts
+        return (rows_w * n_fs, cols_w) if dim == 0 else (rows_w, cols_w * n_fs)
 
     def scratch(*shape, dtype=f32):
         return pltpu.VMEM(shape, dtype)
@@ -1027,45 +1224,46 @@
     dma = pltpu.SemaphoreType.DMA
     channels, lat = cv.shape[1], md.shape[1] * n_tp
     rope = rope_weight.shape[1]
-    others = n_sp - 1
+    couples = n_sp // 2
+    spare = max(couples - 1, 1)
+    count = 10
     return pl.pallas_call(
         functools.partial(fused_kernel, sizes),
-        out_shape=[jax.ShapeDtypeStruct((rows, ho.shape[1] * n_fs), bf16)] * 2,
-        in_specs=[vmem] * 12 + [hbm] * 9,
-        out_specs=[vmem] * 2,
-        scratch_shapes=[
-            scratch(*whole(md), dtype=bf16), scratch(*whole(qd), dtype=bf16),
+        out_shape=jax.ShapeDtypeStruct((rows, ho.shape[1] * n_fs), bf16),
+        in_specs=[hbm] * 21,
+        out_specs=hbm,
+        scratch_shapes=[scratch(*a.shape, dtype=a.dtype) for a in small] + [
+            scratch(*whole(qd), dtype=bf16), scratch(*whole(md), dtype=bf16),
             scratch(*whole(ku), dtype=bf16), scratch(*whole(vu), dtype=bf16),
-            scratch(*whole(qu), dtype=bf16), scratch(*whole(cv), dtype=bf16),
-            scratch(*whole(cg), dtype=bf16), scratch(*whole(ho, 1), dtype=bf16),
+            scratch(*whole(qu), dtype=bf16), scratch(*whole(cv, 0, 2), dtype=bf16),
+            scratch(*whole(cg, 0, 2), dtype=bf16), scratch(*whole(ho, 1), dtype=bf16),
             scratch(*whole(co, 1), dtype=bf16),
-            scratch(rows, model, dtype=bf16), scratch(n_tp, rows, qd.shape[1], dtype=bf16),
-            scratch(n_tp, rows, md.shape[1], dtype=bf16),
+            scratch(2, rows, model, dtype=bf16), scratch(2, rows, model, dtype=bf16),
+            scratch(n_tp, rows, qd.shape[1], dtype=bf16), scratch(rows, qd.shape[1], dtype=bf16),
+            scratch(n_tp, 2, rows, md.shape[1], dtype=bf16),
             scratch(n_sp, lat, rows, dtype=bf16), scratch(n_sp, rope, rows, dtype=bf16),
             scratch(qu.shape[0] * n_fs, rows, dtype=bf16), scratch(qu.shape[1], rows),
             scratch(n_sp, ku.shape[1], rows), scratch(n_sp, vu.shape[1], rows, dtype=bf16),
             scratch(n_sp, rope, rows), scratch(n_sp, 1, rows),
+            scratch(QK_DIM, rows), scratch(QK_DIM, rows),
             scratch(n_sp, rows, rows), scratch(n_sp, rows, rows),
             scratch(vu.shape[1], rows), scratch(rows, channels, dtype=bf16),
-            scratch(rows, channels), scratch(rows, channels),
+            scratch(rows, channels // 2), scratch(rows, channels // 2),
             scratch(rows, ho.shape[1] * n_fs),
+            scratch(rows, channels // 2, dtype=bf16), scratch(rows, channels // 2, dtype=bf16),
             scratch(rows + RIM, channels), scratch(RIM, channels, dtype=bf16),
             scratch(RIM, channels, dtype=bf16), scratch(rows, channels),
             scratch(2 * rows, 128), scratch(2 * rows, 128),
-            dma((9, 2)), dma((9, 2)), dma((9, 2)), dma((9, 2)),
-            dma((9, 3)), dma((9, 3)), dma((9,)), dma((2,)),
-            dma((others,)), dma((others,)), dma((others,)), dma((others,)),
-            dma((others,)), dma((others,)), dma((3,)), dma((3,)), dma((n_fs,)), dma((n_fs,)),
+            *[scratch(rows, ho.shape[1] * n_fs, dtype=bf16)] * 3,
+            dma((count, 2)), dma((count, 2)), dma((count, 2)), dma((count, 2)),
+            dma((count, 3)), dma((count, 3)), dma((count,)), dma((len(small),)), dma((2,)),
+            dma((5,)), dma((6,)), dma((spare, 2, 2)), dma((spare, 2)),
+            dma((couples,)), dma((couples,)), dma((3,)), dma((3,)), dma((n_fs,)), dma((n_fs,)), dma((n_fs,)),
         ],
         compiler_params=pltpu.CompilerParams(
             collective_id=1, has_side_effects=True, vmem_limit_bytes=60 * 1024 * 1024
         ),
-    )(
-        x, mix_gain[None, :], rope_weight.T, taps, channel_gain[None, :], channel_shift[None, :],
-        latent_gain[None, :], memory_gain[None, :], query_gain[:, None], key_gain[:, None],
-        jnp.asarray(cosine), jnp.asarray(sine),
-        md, qd, ku, vu, qu, cv, cg, ho, co,
-    )
+    )(x, *small, qd, md, ku, vu, qu, cv, cg, ho, co)
 
 
 def fused_local(
@@ -1073,14 +1271,14 @@
     latent_gain, memory_gain, query_gain, key_gain, conv_value, conv_gate, conv_kernel,
     channel_gain, channel_shift, heads_out, conv_out,
 ):
-    mine, other = fused_call(
+    mixed = fused_call(
         (lax.axis_size("fs"), lax.axis_size("sp"), lax.axis_size("tp")),
         tokens[0], mix_gain, rope_weight, conv_kernel, channel_gain, channel_shift,
         latent_gain, memory_gain, query_gain, key_gain,
         query_down, memory_down, conv_value, conv_gate,
         query_up, key_up, value_up, heads_out, conv_out,
     )
-    return (mine.astype(jnp.float32) + other.astype(jnp.float32)).astype(jnp.bfloat16)[None]
+    return mixed[None]
 
 
 def solution(mesh):

time: 114 us -> 90.2 us (0.79)
  the two profiles are of different devices: /device:TPU:0 before, /device:TPU:17 now
where the time goes in v2:
time: 90.2 us; the launch traced here: 90 us
  Pallas kernels  87.7 us (97%)
  local copies, waits for them, and re-layouts  2.3 us (3%)
    pallas_call x1, Pallas kernels, fused_call(): pl.pallas_call(functools.partial(fused_kernel, sizes), out_shape=jax.Shap...  87.7 us
    unnamed x1, local copies, waits for them, and re-layouts  2.3 us

profile of v2, /device:TPU:17, one launch (start us, length us, event | category | flops | bytes accessed | tf_op | source)
XLA Modules:
  0.0 90.0 jit_solution(2587693695448095483)
XLA Ops:
  0.0 87.7 %shard_map.199 = bf16[256,2048]{1,0:T(8,128)(2,1)} custom-call(bf16[256,2048]{1,0:T(8,128)(2,1)} %bitcast.11, f32[1,2048]{1,0:T(1,128)} %bitcast.13, bf16[32,2048]{1,0:T(8,128)(2,1)} %bitcast.12, bf16[31,512]{1,0:T(8,128)(2,1)} %taps_hbm.1, f32[1,512]{1,0:T(1,128)} %bitcast.15, f32[1,512]{1,0:T(1,128)} %bitcast.16, f32[6,128]{1,0:T(8,128)} %bitcast.14, ...), custom_call_target="tpu_custom_call" | custom-call | tf_op jit(solution)/shard_map/pallas_call | solution.py:1230
  87.7 2.3 %copy.23 = bf16[1,256,2048]{2,1,0:T(8,128)(2,1)} copy(bf16[1,256,2048]{2,1,0:T(8,128)(2,1)} %bitcast.10) | data formatting | bytes 2097152

commit v3 on v2

--- a/solution.py
+++ b/solution.py
@@ -565,8 +565,8 @@
     )
 
 
-def swapped_rows(count, eighths):
-    return (count * eighths // 8) // 16 * 16
+def swapped_rows(count, part):
+    return (count * part // 16) // 16 * 16
 
 
 def fused_kernel(
@@ -574,14 +574,14 @@
     x_hbm, gain_hbm, rope_hbm, taps_hbm, cgain_hbm, cshift_hbm,
     lgain_hbm, mgain_hbm, qgain_hbm, kgain_hbm, cos_hbm, sin_hbm,
     qd, md, ku, vu, qu, cv, cg, ho, co,
-    out_hbm,
+    mine_hbm, other_hbm,
     gain_ref, rope_ref, taps_ref, cgain_ref, cshift_ref,
     lgain_ref, mgain_ref, qgain_ref, kgain_ref, cos_ref, sin_ref,
     qd_all, md_all, ku_all, vu_all, qu_all, cv_all, cg_all, ho_all, co_all,
-    x_all, normed, lq_all, lq_out, lm_all, mem_all, rr_all, qn_t, q_t, k_t, v_t,
+    x_all, normed, lq_all, lm_all, mem_all, rr_all, qn_t, q_t, k_t, v_t,
     turned, ropesq, qcol, kcol, bias, scores,
-    att_t, conv_s, acc_v, acc_g, acc_out, gate_out, gate_in, ext, tail, rim, sums, stats, stats_all,
-    mine_ref, other_ref, whole_ref,
+    att_t, att_out, att_all, conv_s, acc_v, acc_out, gate_out, gate_in, ext, rim_out, rim, sums, stats, stats_all,
+    mine_ref,
     send_d, recv_d, send_r, recv_r, send_z, recv_z, local_sem, small_sem, rim_sem, x_sem,
     part_sem, sp_send, sp_recv, fw_send, fw_recv, tp_send, tp_recv, out_send, out_recv, store_sem,
 ):
@@ -603,11 +603,12 @@
                 barrier, inc=1, device_id={axis: lax.rem(at + k, count)}, device_id_type=MESH_ID
             )
 
+    slots = 3
     rows = x_hbm.shape[0]
     x_own = pltpu.make_async_copy(x_hbm, x_all.at[parity], x_sem.at[0])
     x_own.start()
     small = [
-        pltpu.make_async_copy(source, landing, small_sem.at[i])
+        pltpu.make_async_copy(source, landing, small_sem.at[i % slots])
         for i, (source, landing) in enumerate((
             (gain_hbm, gain_ref), (rope_hbm, rope_ref), (taps_hbm, taps_ref),
             (cgain_hbm, cgain_ref), (cshift_hbm, cshift_ref), (lgain_hbm, lgain_ref),
@@ -615,7 +616,7 @@
             (cos_hbm, cos_ref), (sin_hbm, sin_ref),
         ))
     ]
-    for copy in small:
+    for copy in small[:slots]:
         copy.start()
 
     def remote(source, landing, send, recv, device):
@@ -637,11 +638,12 @@
     far = lax.rem(near_x + 2, 4)
     sources = [near_x, near_y]
 
-    def job(a, shard, whole, swap, dim=0, first=0, count=None):
+    def job(a, shard, whole, swap=None, dim=0, first=0, count=None):
         depth, cols = shard.shape
         count = depth if count is None else count
-        less = swapped_rows(count, swap)
-        kept = count - less
+        lane, mine, lacking, giving = swap or (0, 0, 0, 0)
+        lack, give = swapped_rows(count, lacking), swapped_rows(count, giving)
+        kept = count - lack
 
         def place(owner, start, size):
             if dim == 0:
@@ -651,11 +653,11 @@
                 pl.ds(pl.multiple_of(owner * cols, 128), cols),
             ]
 
-        start = first + parity * less
+        start = first + mine * lack
         direct = [
             remote(
-                shard.at[pl.ds(pl.multiple_of(start, 16), kept), :], place(f, start, kept),
-                send_d.at[a, k], recv_d.at[a, k], {"fs": target},
+                shard.at[pl.ds(start, kept), :], place(f, start, kept),
+                send_d.at[a % slots, k], recv_d.at[a, k], {"fs": target},
             )
             for k, target in enumerate(sources)
         ]
@@ -665,30 +667,54 @@
             (near_y, near_x, start, half), (near_x, near_y, start + half, kept - half)
         )):
             piece = place(owner, begin, size)
-            relays.append(remote(piece, piece, send_r.at[a, k], recv_r.at[a, k], {"fs": target}))
-        across = []
-        if less:
+            relays.append(remote(
+                piece, piece, send_r.at[a % slots, k], recv_r.at[a, k], {"fs": target}
+            ))
+        gives, lacks = [], []
+        if swap:
             for k, owner in enumerate(sources + [far]):
-                piece = place(owner, first + parity * kept, less)
-                across.append(remote(piece, piece, send_z.at[a, k], recv_z.at[a, k], partner))
+                sems = (send_z.at[lane, k], recv_z.at[lane, k], partner)
+                if give:
+                    piece = place(owner, first + mine * (count - give), give)
+                    gives.append(remote(piece, piece, *sems))
+                if lack:
+                    piece = place(owner, first + (1 - mine) * kept, lack)
+                    lacks.append(remote(piece, piece, *sems))
         own = pltpu.make_async_copy(
-            shard.at[pl.ds(first, count), :], place(f, first, count), local_sem.at[a]
+            shard.at[pl.ds(first, count), :], place(f, first, count), local_sem.at[a % slots]
         )
-        return direct, relays, across, own
+        return direct, relays, gives, own, lacks
+
+    def half_columns(shard):
+        width = shard.shape[1] // 2
+        return shard.at[:, pl.ds(pl.multiple_of(parity * width, 128), width)]
 
     wide = cv.shape[1] // 2
     side = pl.ds(pl.multiple_of(parity * wide, 128), wide)
     half_rows = ho.shape[0] // 2
+    last_rows = half_rows // 4
+
+    def swapping(lane, even_lacks, odd_lacks, *rest):
+        shard, whole, *rest = rest
+        return [
+            (even, shard, whole, (lane, 0, even_lacks, odd_lacks), *rest),
+            (odd, shard, whole, (lane, 1, odd_lacks, even_lacks), *rest),
+        ]
+
     plan = [
-        [(even, qd, qd_all, 0), (odd, md, md_all, 0)],
-        [(None, ku, ku_all, 4)], [(None, vu, vu_all, 4)], [(None, qu, qu_all, 4)],
-        [(None, cv.at[:, side], cv_all, 0)], [(None, cg.at[:, side], cg_all, 0)],
-        [(None, ho, ho_all, 4, 1, 0, half_rows)], [(None, ho, ho_all, 4, 1, half_rows, half_rows)],
-        [(None, co, co_all, 3, 1, 0, half_rows)], [(None, co, co_all, 0, 1, half_rows, half_rows)],
+        [(even, qd, qd_all), (odd, md, md_all)],
+        [(None, half_columns(ku), ku_all)], [(None, half_columns(vu), vu_all)],
+        [(None, half_columns(qu), qu_all)],
+        swapping(0, 8, 8, ho, ho_all, 1, 0, half_rows),
+        [(None, half_columns(cv), cv_all)], [(None, half_columns(cg), cg_all)],
+        swapping(1, 8, 8, ho, ho_all, 1, half_rows, half_rows),
+        swapping(2, 6, 4, co, co_all, 1, 0, half_rows),
+        [(None, co, co_all, None, 1, half_rows, half_rows - last_rows)],
+        [(None, co, co_all, None, 1, 2 * half_rows - last_rows, last_rows)],
     ]
     jobs = [[(who[0], job(a, *who[1:])) for who in group] for a, group in enumerate(plan)]
     last = len(jobs) - 1
-    ahead = 3
+    lanes = [a for a, group in enumerate(plan) if len(group[0]) > 3 and group[0][3]]
 
     def each(a, action):
         for condition, parts in jobs[a]:
@@ -697,12 +723,22 @@
             else:
                 pl.when(condition)(functools.partial(action, parts))
 
+    def sent(a, kind):
+        def go(parts):
+            for copy in parts[kind]:
+                copy.wait_send()
+
+        if a >= 0:
+            each(a, go)
+
     def begin_array(a):
         def start(parts):
             for copy in parts[0]:
                 copy.start()
+            parts[3].start()
 
         if a <= last:
+            sent(a - slots, 0)
             each(a, start)
 
     def finish_far(a):
@@ -720,6 +756,7 @@
             with jax.named_scope(f"direct_{a}"):
                 for copy in parts[0]:
                     copy.wait_recv()
+                parts[3].wait()
             for copy in parts[1]:
                 copy.start()
 
@@ -727,15 +764,16 @@
             for copy in parts[2][: len(sources)]:
                 copy.start()
 
+        sent(a - slots, 1)
         each(a, go)
-        begin_array(a + ahead)
-        each(a, swap)
+        begin_array(a + slots)
+        if a in lanes:
+            each(a, swap)
 
     def complete(a):
         def go(parts):
             with jax.named_scope(f"across_{a}"):
-                parts[3].wait()
-                for copy in parts[2]:
+                for copy in parts[4]:
                     copy.wait_recv()
 
         each(a, go)
@@ -743,13 +781,15 @@
     with jax.named_scope("entry"):
         pl.semaphore_wait(barrier, n_fs + n_sp + n_tp - 3)
     x_send.start()
-    for a in range(ahead):
+    for a in range(slots):
         begin_array(a)
-    for a in range(last + 1):
-        each(a, lambda parts: parts[3].start())
     with jax.named_scope("small_wait"):
-        for copy in small:
-            copy.wait()
+        for r in range(0, len(small), slots):
+            if r:
+                for copy in small[r : r + slots]:
+                    copy.start()
+            for copy in small[r : r + slots]:
+                copy.wait()
         x_own.wait()
 
     part = 32
@@ -784,14 +824,11 @@
         mem_all[j] = jnp.zeros(mem_all.shape[1:], jnp.bfloat16)
         rr_all[j] = jnp.zeros(rr_all.shape[1:], jnp.bfloat16)
 
-    @pl.when(even)
-    def _():
-        mem_all[s + 1] = jnp.zeros(mem_all.shape[1:], jnp.bfloat16)
-
     @pl.loop(0, n_sp)
     def _(j):
-        key_at = j * rows + lax.broadcasted_iota(jnp.int32, (rows, rows), 0)
-        query_at = s * rows + lax.broadcasted_iota(jnp.int32, (rows, rows), 1)
+        shape = (rows, 2 * rows)
+        key_at = j * rows + lax.broadcasted_iota(jnp.int32, shape, 0)
+        query_at = 2 * couple * rows + lax.broadcasted_iota(jnp.int32, shape, 1)
         bias[j] = jnp.where(
             lax.div(key_at, SEG) <= lax.div(query_at, SEG), 0.0, masked_score
         )
@@ -807,22 +844,13 @@
     tick(2)
     finish_far(0)
 
-    depth = qd.shape[0]
-
-    def project(weight, b, acc):
-        acc[...] = jnp.zeros_like(acc)
-
-        @pl.loop(0, n_fs)
-        def _(i):
-            at = pl.ds(pl.multiple_of(i * depth, depth), depth)
-            acc[...] += jnp.dot(
-                normed[b, :, at], weight[at, :], preferred_element_type=jnp.float32
-            )
+    def project(weight, b):
+        return jnp.dot(normed[b], weight[...], preferred_element_type=jnp.float32)
 
     lat = md.shape[1]
     lat_q = qd.shape[1]
     held = pl.ds(pl.multiple_of(t * lat, lat), lat)
-    query_across = remote(lq_out, lq_all.at[t], part_sem.at[0], part_sem.at[1], partner)
+    query_across = remote(lq_all.at[t], lq_all.at[t], part_sem.at[0], part_sem.at[1], partner)
     query_copy = remote(lq_all.at[t], lq_all.at[t], tp_send.at[0], tp_recv.at[0], twin)
     memory_copy = remote(lm_all.at[t], lm_all.at[t], tp_send.at[1], tp_recv.at[1], twin)
     stat_copy = remote(stats, stats_all, tp_send.at[2], tp_recv.at[2], twin)
@@ -832,18 +860,15 @@
 
     @pl.when(even)
     def _():
-        project(qd_all, 1, acc_out.at[:, pl.ds(0, lat_q)])
-        lq_out[...] = acc_out[:, :lat_q].astype(jnp.bfloat16)
+        for b in range(2):
+            lq_all[t, b] = project(qd_all, b).astype(jnp.bfloat16)
         query_across.start()
-        project(qd_all, 0, acc_out.at[:, pl.ds(0, lat_q)])
-        lq_all[t] = acc_out[:, :lat_q].astype(jnp.bfloat16)
         query_copy.start()
 
     @pl.when(odd)
     def _():
         for b in range(2):
-            project(md_all, b, acc_v.at[:, pl.ds(0, lat)])
-            lm_all[t, b] = acc_v[:, :lat].astype(jnp.bfloat16)
+            lm_all[t, b] = project(md_all, b).astype(jnp.bfloat16)
         memory_copy.start()
 
     tick(3)
@@ -859,13 +884,10 @@
                 shaped = (pieces[g] * scale * gain_at(g * width, width)).astype(jnp.bfloat16)
                 put(g * width, width, at, shaped.astype(jnp.float32).T.astype(jnp.bfloat16))
 
-    mine_block = mem_all.at[s, held, :]
-    back = remote(
-        mem_all.at[2 * couple, held, :], mem_all.at[2 * couple, held, :],
-        part_sem.at[4], part_sem.at[5], partner,
-    )
-    back_forward = remote(mine_block, mine_block, fw_send.at[couples - 1], fw_recv.at[couples - 1], twin)
     pair = pl.ds(2 * couple, 2)
+    both = mem_all.at[pair, held, :]
+    back = remote(both, both, part_sem.at[4], part_sem.at[5], partner)
+    back_forward = remote(both, both, fw_send.at[couples - 1], fw_recv.at[couples - 1], twin)
     onward, forwards = [], []
     for d in range(1, couples):
         group = []
@@ -905,56 +927,33 @@
                     for copy in onward[d - 1][e]:
                         copy.start()
         back.start()
+
+    finish_far(1)
+    tick(4)
+    finish_far(2)
+
+    @pl.when(even)
+    def _():
+        with jax.named_scope("back_wait"):
+            back.wait_recv()
+        back_forward.start()
+
+    tick(5)
+    finish_far(3)
+
+    @pl.when(odd)
+    def _():
         with jax.named_scope("query_across"):
             query_across.wait_recv()
         query_copy.start()
 
-    finish_far(1)
-    tick(4)
-
-    def put_query(begin, width, at, piece):
-        qn_t[begin : begin + width, at] = piece
-
-    with jax.named_scope("query_wait"):
-        query_copy.wait_recv()
-    normed_columns(
-        lambda g, at: lq_all[g, at, :], lat_q,
-        lambda begin, width: jnp.concatenate(
-            [lgain_ref[r : r + 1, :] for r in range(begin // 128, (begin + width) // 128)], axis=1
-        ),
-        put_query,
-    )
-    finish_far(2)
-
-    @pl.when(even)
-    def _():
-        with jax.named_scope("back_wait"):
-            back.wait_recv()
-        back_forward.start()
-
-    for d in range(1, couples):
-        @pl.when(couple >= d)
-        def _(d=d):
-            with jax.named_scope(f"behind_{d}"):
-                for copy in onward[d - 1][0]:
-                    copy.wait_recv()
-            forwards[d - 1].start()
-    complete(1)
-    complete(2)
 
     @pl.when(even)
     def _():
         with jax.named_scope("back_forward"):
             back_forward.wait_recv()
 
-    for d in range(1, couples):
-        @pl.when(couple >= d)
-        def _(d=d):
-            with jax.named_scope(f"forward_{d}"):
-                forwards[d - 1].wait_recv()
-
-    @pl.loop(0, n_sp)
-    def _(j):
+    def expand(j):
         k_t[j] = dot_heads(ku_all[...], mem_all[j])
         v_t[j] = dot_heads(vu_all[...], mem_all[j]).astype(jnp.bfloat16)
         shared = rr_all[j].astype(jnp.float32)
@@ -967,13 +966,40 @@
             [front * cosine - back_half * sine, front * sine + back_half * cosine], axis=0
         )
 
-    tick(5)
-    finish_far(3)
+    pl.loop(2 * couple, n_sp)(expand)
+    for d in range(1, couples):
+        @pl.when(couple >= d)
+        def _(d=d):
+            with jax.named_scope(f"behind_{d}"):
+                for copy in onward[d - 1][0]:
+                    copy.wait_recv()
+            forwards[d - 1].start()
     tick(6)
-    complete(3)
+    finish_far(4)
+    with jax.named_scope("query_wait"):
+        query_copy.wait_recv()
+    for b in range(2):
+        def put_query(begin, width, at, piece, b=b):
+            at = pl.ds(pl.multiple_of(b * rows + at.start, 128), at.size)
+            qn_t[begin : begin + width, at] = piece
+
+        normed_columns(
+            lambda g, at, b=b: lq_all[g, b, at, :], lat_q,
+            lambda begin, width: jnp.concatenate(
+                [lgain_ref[r : r + 1, :] for r in range(begin // 128, (begin + width) // 128)],
+                axis=1,
+            ),
+            put_query,
+        )
+    for d in range(1, couples):
+        @pl.when(couple >= d)
+        def _(d=d):
+            with jax.named_scope(f"forward_{d}"):
+                forwards[d - 1].wait_recv()
+    pl.loop(0, 2 * couple)(expand)
     q_t[...] = dot_heads(qu_all[...], qn_t[...])
-    heads = qu.shape[1] // QK_DIM
-    here = pl.ds(pl.multiple_of(s * rows, rows), rows)
+    heads = qu.shape[1] // 2 // QK_DIM
+    here = pl.ds(pl.multiple_of(2 * couple * rows, rows), 2 * rows)
     score_scale = QK_DIM ** (-0.5)
 
     def head(h):
@@ -991,7 +1017,7 @@
         ).astype(jnp.bfloat16)
         krow = pl.ds(pl.multiple_of(h * QK_NOPE, QK_NOPE), QK_NOPE)
         vrow = pl.ds(pl.multiple_of(h * V_DIM, V_DIM), V_DIM)
-        top = jnp.full((1, rows), masked_score, jnp.float32)
+        top = jnp.full((1, 2 * rows), masked_score, jnp.float32)
         for j in range(n_sp):
             nope = k_t[j, krow, :]
             scale = lax.rsqrt(
@@ -1003,8 +1029,8 @@
             block = dot_heads(key, q) + bias[j]
             scores[j] = block
             top = jnp.maximum(top, jnp.max(block, axis=0, keepdims=True))
-        total = jnp.zeros((1, rows), jnp.float32)
-        summed = jnp.zeros((V_DIM, rows), jnp.float32)
+        total = jnp.zeros((1, 2 * rows), jnp.float32)
+        summed = jnp.zeros((V_DIM, 2 * rows), jnp.float32)
         for j in range(n_sp):
             weight = jnp.exp((scores[j] - top) * score_scale)
             total = total + jnp.sum(weight, axis=0, keepdims=True)
@@ -1015,48 +1041,78 @@
         att_t[vrow, :] = summed / total
 
     pl.loop(0, heads // 2)(head)
-    finish_far(4)
     tick(7)
+    finish_far(5)
+    for b in range(2):
+        acc_v[b] = project(cv_all, b)
     pl.loop(heads // 2, heads)(head)
-    finish_far(5)
-    complete(4)
-    complete(5)
-    for other_block in (True, False):
-        b = 1 - parity if other_block else parity
-        project(cv_all, b, acc_v)
-        project(cg_all, b, acc_g)
-        gated = (acc_v[...] * jax.nn.sigmoid(acc_g[...])).astype(jnp.bfloat16)
-        if other_block:
-            gate_out[...] = gated
-            gate_across.start()
-            tick(8)
-            finish_far(6)
-        else:
-            ext[pl.ds(RIM, rows), side] = gated.astype(jnp.float32)
-    with jax.named_scope("gate_wait"):
-        gate_across.wait_recv()
-    ext[
-        pl.ds(RIM, rows), pl.ds(pl.multiple_of((1 - parity) * wide, 128), wide)
-    ] = gate_in[...].astype(jnp.float32)
-
-    tail[...] = ext[pl.ds(rows, RIM), :].astype(jnp.bfloat16)
-    rim_copy = remote(
-        tail, rim, rim_sem.at[0], rim_sem.at[1], {"sp": lax.rem(s + 1, n_sp)}
-    )
-
-    @pl.when(s < n_sp - 1)
-    def _():
-        rim_copy.start()
-
-    @pl.when(s > 0)
+    value_rows = heads * V_DIM
+    own_rows = pl.ds(pl.multiple_of(parity * value_rows, value_rows), value_rows)
+    their_lanes = pl.ds(pl.multiple_of((1 - parity) * rows, rows), rows)
+    own_lanes = pl.ds(pl.multiple_of(parity * rows, rows), rows)
+    att_across = remote(
+        att_out, att_all.at[own_rows, :], part_sem.at[6], part_sem.at[7], partner
+    )
+    att_out[...] = att_t[:, their_lanes].astype(jnp.bfloat16)
+    att_across.start()
+    att_all[own_rows, :] = att_t[:, own_lanes].astype(jnp.bfloat16)
+    tick(8)
+    finish_far(6)
+    opposite = pl.ds(pl.multiple_of((1 - parity) * wide, 128), wide)
+    body_rows, halo = pl.ds(RIM, rows), pl.ds(0, RIM)
+
+    def gate(b):
+        gates = project(cg_all, b)
+        return (acc_v[b] * jax.nn.sigmoid(gates)).astype(jnp.bfloat16)
+
+    end = slice(rows - RIM, rows)
+    later_rim = remote(
+        rim_out, rim.at[parity], rim_sem.at[0], rim_sem.at[1 + parity],
+        {"sp": 2 * lax.rem(couple + 1, couples)},
+    )
+    has_later, has_earlier = couple < couples - 1, jnp.logical_and(even, couple > 0)
+    lower = gate(0)
+
+    @pl.when(even)
+    def _():
+        ext[body_rows, side] = lower.astype(jnp.float32)
+        ext[halo, :] = jnp.zeros((RIM, ext.shape[1]), jnp.float32)
+        gate_out[halo, :] = lower[end]
+
+    @pl.when(odd)
+    def _():
+        gate_out[halo, :] = jnp.zeros((RIM, wide), jnp.bfloat16)
+        gate_out[body_rows, :] = lower
+        gate_across.start()
+        ext[halo, side] = lower[end].astype(jnp.float32)
+
+    upper = gate(1)
+    rim_out[...] = upper[end]
+
+    @pl.when(has_later)
+    def _():
+        later_rim.start()
+
+    @pl.when(even)
+    def _():
+        gate_out[body_rows, :] = upper
+        gate_across.start()
+
+    @pl.when(odd)
+    def _():
+        ext[body_rows, side] = upper.astype(jnp.float32)
+
+    tick(9)
+
+    @pl.when(has_earlier)
     def _():
         with jax.named_scope("rim_wait"):
-            rim_copy.wait_recv()
-        ext[pl.ds(0, RIM), :] = rim[...].astype(jnp.float32)
-
-    @pl.when(s == 0)
-    def _():
-        ext[pl.ds(0, RIM), :] = jnp.zeros((RIM, ext.shape[1]), jnp.float32)
+            for g in range(2):
+                remote(
+                    rim_out, rim.at[g], rim_sem.at[0], rim_sem.at[1 + g], partner
+                ).wait_recv()
+        for g in range(2):
+            ext[halo, g * wide : (g + 1) * wide] = rim[g].astype(jnp.float32)
 
     tap_count = taps_ref.shape[0]
     block = 64
@@ -1072,11 +1128,20 @@
                 ] * taps[j : j + 1, :]
             sums[pl.ds(r, block), cols] = total
 
-    tiles = ext.shape[1] // 128
-    pl.loop(0, tiles // 2)(convolve)
+    tiles = wide // 128
+    pl.loop(parity * tiles, (parity + 1) * tiles)(convolve)
+    with jax.named_scope("gate_wait"):
+        gate_across.wait_recv()
+    ext[body_rows, opposite] = gate_in[body_rows, :].astype(jnp.float32)
+
+    @pl.when(odd)
+    def _():
+        ext[halo, opposite] = gate_in[halo, :].astype(jnp.float32)
+
     finish_far(7)
-    pl.loop(tiles // 2, tiles)(convolve)
-    tick(9)
+    pl.loop((1 - parity) * tiles, (2 - parity) * tiles)(convolve)
+    finish_far(8)
+    tick(10)
 
     @pl.loop(0, rows // part)
     def _(i):
@@ -1090,17 +1155,22 @@
         )
 
     stat_copy.start()
-    finish_far(8)
-    complete(6)
-    complete(7)
-    att = att_t[...].T.astype(jnp.bfloat16)
+    with jax.named_scope("att_wait"):
+        att_across.wait_recv()
+    att = att_all[...].astype(jnp.float32).T.astype(jnp.bfloat16)
     span = ho.shape[1]
 
-    @pl.loop(0, n_fs)
-    def _(i):
-        cols = pl.ds(pl.multiple_of(i * span, span), span)
-        acc_out[:, cols] = jnp.dot(att, ho_all[:, cols], preferred_element_type=jnp.float32)
-
+    def gain_rows(left, weight, begin, size=half_rows, first=False):
+        band = slice(begin, begin + size)
+
+        @pl.loop(0, n_fs)
+        def _(i):
+            cols = pl.ds(pl.multiple_of(i * span, span), span)
+            product = jnp.dot(left[:, band], weight[band, cols], preferred_element_type=jnp.float32)
+            acc_out[:, cols] = product if first else acc_out[:, cols] + product
+
+    complete(4)
+    gain_rows(att, ho_all, 0, first=True)
     with jax.named_scope("stat_wait"):
         stat_copy.wait_recv()
     channels = ext.shape[1] * n_tp
@@ -1119,39 +1189,40 @@
             shaped * cgain_ref[...] + cshift_ref[...]
         ).astype(jnp.bfloat16)
 
-    finish_far(last)
+    complete(7)
+    gain_rows(att, ho_all, half_rows)
     complete(8)
-
-    @pl.loop(0, n_fs)
-    def _(i):
-        cols = pl.ds(pl.multiple_of(i * span, span), span)
-        acc_out[:, cols] += jnp.dot(
-            conv_s[:, :half_rows], co_all[:half_rows, cols], preferred_element_type=jnp.float32
-        )
-
-    complete(last)
-    outs = []
-    for i in range(n_fs):
-        cols = slice(i * span, (i + 1) * span)
+    gain_rows(conv_s, co_all, 0)
+    finish_far(9)
+    gain_rows(conv_s, co_all, half_rows, half_rows - last_rows)
+    rest = slice(2 * half_rows - last_rows, 2 * half_rows)
+    outs, stores = [], []
+    for i, owner in enumerate([f, near_x, near_y, far]):
+        cols = pl.ds(pl.multiple_of(owner * span, span), span)
         outs.append(remote(
-            mine_ref.at[:, cols], other_ref.at[:, cols], out_send.at[i], out_recv.at[i], twin
+            mine_ref.at[:, cols], other_hbm.at[:, cols], out_send.at[i], out_recv.at[i], twin
         ))
+        stores.append(pltpu.make_async_copy(
+            mine_ref.at[:, cols], mine_hbm.at[:, cols], store_sem.at[i]
+        ))
+        if i == n_fs - 1:
+            finish_far(last)
         mine_ref[:, cols] = (
             acc_out[:, cols]
             + jnp.dot(
-                conv_s[:, half_rows:], co_all[half_rows:, cols],
+                conv_s[:, rest], co_all[rest, cols],
                 preferred_element_type=jnp.float32,
             )
         ).astype(jnp.bfloat16)
         outs[i].start()
-
-    def drain(parts):
-        for copy in parts[0] + parts[1] + parts[2]:
-            copy.wait_send()
-
-    for a in range(last + 1):
-        each(a, drain)
-    for copy in (x_send, x_forward, query_copy, stat_copy, gate_across):
+        stores[i].start()
+
+    for a in range(last + 1 - slots, last + 1):
+        sent(a, 0)
+        sent(a, 1)
+    for a in lanes:
+        sent(a, 2)
+    for copy in (x_send, x_forward, query_copy, stat_copy, gate_across, att_across):
         copy.wait_send()
 
     @pl.when(even)
@@ -1175,27 +1246,57 @@
         def _(d=d):
             forwards[d - 1].wait_send()
 
-    @pl.when(s < n_sp - 1)
-    def _():
-        rim_copy.wait_send()
-
-    stores = []
-    for i in range(n_fs):
-        cols = slice(i * span, (i + 1) * span)
-        with jax.named_scope(f"out_wait_{i}"):
-            outs[i].wait_recv()
-        whole_ref[:, cols] = (
-            mine_ref[:, cols].astype(jnp.float32) + other_ref[:, cols].astype(jnp.float32)
+    @pl.when(has_later)
+    def _():
+        later_rim.wait_send()
+
+    with jax.named_scope("out_wait"):
+        for copy in outs + stores:
+            copy.wait()
+
+
+def join_kernel(mine_hbm, other_hbm, out_hbm, mine, other, whole, loads, stores):
+    rows = mine.shape[0]
+    pieces = loads.shape[0]
+    step = rows // pieces
+
+    def copies(i):
+        at = pl.ds(i * step, step)
+        return (
+            pltpu.make_async_copy(mine_hbm.at[at, :], mine.at[at, :], loads.at[i, 0]),
+            pltpu.make_async_copy(other_hbm.at[at, :], other.at[at, :], loads.at[i, 1]),
+            pltpu.make_async_copy(whole.at[at, :], out_hbm.at[at, :], stores.at[i]),
+        )
+
+    plan = [copies(i) for i in range(pieces)]
+    for one, two, _ in plan:
+        one.start()
+        two.start()
+    for i, (one, two, back) in enumerate(plan):
+        one.wait()
+        two.wait()
+        at = pl.ds(i * step, step)
+        whole[at, :] = (
+            mine[at, :].astype(jnp.float32) + other[at, :].astype(jnp.float32)
         ).astype(jnp.bfloat16)
-        stores.append(pltpu.make_async_copy(
-            whole_ref.at[:, cols], out_hbm.at[:, cols], store_sem.at[i]
-        ))
-        stores[i].start()
-    with jax.named_scope("store_wait"):
-        for copy in outs:
-            copy.wait_send()
-        for copy in stores:
-            copy.wait()
+        back.start()
+    for _, _, back in plan:
+        back.wait()
+
+
+def join(mine, other):
+    pieces = 4
+    buffer = pltpu.VMEM(mine.shape, mine.dtype)
+    dma = pltpu.SemaphoreType.DMA
+    hbm = pl.BlockSpec(memory_space=pl.ANY)
+    return pl.pallas_call(
+        join_kernel,
+        out_shape=jax.ShapeDtypeStruct(mine.shape, mine.dtype),
+        in_specs=[hbm] * 2,
+        out_specs=hbm,
+        scratch_shapes=[buffer] * 3 + [dma((pieces, 2)), dma((pieces,))],
+        compiler_params=pltpu.CompilerParams(vmem_limit_bytes=60 * 1024 * 1024),
+    )(mine, other)
 
 
 def fused_call(
@@ -1226,38 +1327,41 @@
     rope = rope_weight.shape[1]
     couples = n_sp // 2
     spare = max(couples - 1, 1)
-    count = 10
+    count, slots = 11, 3
     return pl.pallas_call(
         functools.partial(fused_kernel, sizes),
-        out_shape=jax.ShapeDtypeStruct((rows, ho.shape[1] * n_fs), bf16),
+        out_shape=[jax.ShapeDtypeStruct((rows, ho.shape[1] * n_fs), bf16)] * 2,
         in_specs=[hbm] * 21,
-        out_specs=hbm,
+        out_specs=[hbm] * 2,
         scratch_shapes=[scratch(*a.shape, dtype=a.dtype) for a in small] + [
             scratch(*whole(qd), dtype=bf16), scratch(*whole(md), dtype=bf16),
-            scratch(*whole(ku), dtype=bf16), scratch(*whole(vu), dtype=bf16),
-            scratch(*whole(qu), dtype=bf16), scratch(*whole(cv, 0, 2), dtype=bf16),
+            scratch(*whole(ku, 0, 2), dtype=bf16), scratch(*whole(vu, 0, 2), dtype=bf16),
+            scratch(*whole(qu, 0, 2), dtype=bf16), scratch(*whole(cv, 0, 2), dtype=bf16),
             scratch(*whole(cg, 0, 2), dtype=bf16), scratch(*whole(ho, 1), dtype=bf16),
             scratch(*whole(co, 1), dtype=bf16),
             scratch(2, rows, model, dtype=bf16), scratch(2, rows, model, dtype=bf16),
-            scratch(n_tp, rows, qd.shape[1], dtype=bf16), scratch(rows, qd.shape[1], dtype=bf16),
+            scratch(n_tp, 2, rows, qd.shape[1], dtype=bf16),
             scratch(n_tp, 2, rows, md.shape[1], dtype=bf16),
             scratch(n_sp, lat, rows, dtype=bf16), scratch(n_sp, rope, rows, dtype=bf16),
-            scratch(qu.shape[0] * n_fs, rows, dtype=bf16), scratch(qu.shape[1], rows),
-            scratch(n_sp, ku.shape[1], rows), scratch(n_sp, vu.shape[1], rows, dtype=bf16),
+            scratch(qu.shape[0] * n_fs, 2 * rows, dtype=bf16), scratch(qu.shape[1] // 2, 2 * rows),
+            scratch(n_sp, ku.shape[1] // 2, rows),
+            scratch(n_sp, vu.shape[1] // 2, rows, dtype=bf16),
             scratch(n_sp, rope, rows), scratch(n_sp, 1, rows),
-            scratch(QK_DIM, rows), scratch(QK_DIM, rows),
-            scratch(n_sp, rows, rows), scratch(n_sp, rows, rows),
-            scratch(vu.shape[1], rows), scratch(rows, channels, dtype=bf16),
-            scratch(rows, channels // 2), scratch(rows, channels // 2),
+            scratch(QK_DIM, 2 * rows), scratch(QK_DIM, rows),
+            scratch(n_sp, rows, 2 * rows), scratch(n_sp, rows, 2 * rows),
+            scratch(vu.shape[1] // 2, 2 * rows), scratch(vu.shape[1] // 2, rows, dtype=bf16),
+            scratch(vu.shape[1], rows, dtype=bf16), scratch(rows, channels, dtype=bf16),
+            scratch(2, rows, channels // 2),
             scratch(rows, ho.shape[1] * n_fs),
-            scratch(rows, channels // 2, dtype=bf16), scratch(rows, channels // 2, dtype=bf16),
-            scratch(rows + RIM, channels), scratch(RIM, channels, dtype=bf16),
-            scratch(RIM, channels, dtype=bf16), scratch(rows, channels),
+            scratch(rows + RIM, channels // 2, dtype=bf16),
+            scratch(rows + RIM, channels // 2, dtype=bf16),
+            scratch(rows + RIM, channels), scratch(RIM, channels // 2, dtype=bf16),
+            scratch(2, RIM, channels // 2, dtype=bf16), scratch(rows, channels),
             scratch(2 * rows, 128), scratch(2 * rows, 128),
-            *[scratch(rows, ho.shape[1] * n_fs, dtype=bf16)] * 3,
-            dma((count, 2)), dma((count, 2)), dma((count, 2)), dma((count, 2)),
-            dma((count, 3)), dma((count, 3)), dma((count,)), dma((len(small),)), dma((2,)),
-            dma((5,)), dma((6,)), dma((spare, 2, 2)), dma((spare, 2)),
+            scratch(rows, ho.shape[1] * n_fs, dtype=bf16),
+            dma((slots, 2)), dma((count, 2)), dma((slots, 2)), dma((count, 2)),
+            dma((slots, 3)), dma((slots, 3)), dma((slots,)), dma((slots,)), dma((3,)),
+            dma((5,)), dma((8,)), dma((spare, 2, 2)), dma((spare, 2)),
             dma((couples,)), dma((couples,)), dma((3,)), dma((3,)), dma((n_fs,)), dma((n_fs,)), dma((n_fs,)),
         ],
         compiler_params=pltpu.CompilerParams(
@@ -1271,14 +1375,14 @@
     latent_gain, memory_gain, query_gain, key_gain, conv_value, conv_gate, conv_kernel,
     channel_gain, channel_shift, heads_out, conv_out,
 ):
-    mixed = fused_call(
+    mine, other = fused_call(
         (lax.axis_size("fs"), lax.axis_size("sp"), lax.axis_size("tp")),
         tokens[0], mix_gain, rope_weight, conv_kernel, channel_gain, channel_shift,
         latent_gain, memory_gain, query_gain, key_gain,
         query_down, memory_down, conv_value, conv_gate,
         query_up, key_up, value_up, heads_out, conv_out,
     )
-    return mixed[None]
+    return join(mine, other)[None]
 
 
 def solution(mesh):

time: 90.2 us -> 79.1 us (0.88)
  the two profiles are of different devices: /device:TPU:17 before, /device:TPU:0 now
where the time goes in v3:
time: 79.1 us; the launch traced here: 78.8 us
  Pallas kernels  78.8 us (100%)
    pallas_call x1, Pallas kernels, fused_call(): pl.pallas_call(functools.partial(fused_kernel, sizes), out_shape=[jax.Sha...  76.5 us
    pallas_call x1, Pallas kernels, join(): pl.pallas_call(join_kernel, out_shape=jax.ShapeDtypeStruct(mine.shape, mi...  2.37 us

profile of v3, /device:TPU:0, one launch (start us, length us, event | category | flops | bytes accessed | tf_op | source)
XLA Modules:
  0.0 78.8 jit_solution(5980018967865958834)
XLA Ops:
  0.0 76.5 %shard_map.199 = (bf16[256,2048]{1,0:T(8,128)(2,1)}, bf16[256,2048]{1,0:T(8,128)(2,1)}) custom-call(bf16[256,2048]{1,0:T(8,128)(2,1)} %bitcast.10, f32[1,2048]{1,0:T(1,128)} %bitcast.12, bf16[32,2048]{1,0:T(8,128)(2,1)} %bitcast.11, bf16[31,512]{1,0:T(8,128)(2,1)} %taps_hbm.1, f32[1,512]{1,0:T(1,128)} %bitcast.14, f32[1,512]{1,0:T(1,128)} %bitcast.15, ...), custom_call_target="tpu_custom_call" | custom-call | tf_op jit(solution)/shard_map/pallas_call | solution.py:1331
  76.5 2.4 %shard_map.200 = bf16[256,2048]{1,0:T(8,128)(2,1)} custom-call(bf16[256,2048]{1,0:T(8,128)(2,1)} %get-tuple-element.7.mine_hbm, bf16[256,2048]{1,0:T(8,128)(2,1)} %get-tuple-element.8.other_hbm), custom_call_target="tpu_custom_call" | custom-call | tf_op jit(solution)/shard_map/pallas_call | solution.py:1292

commit v4 on v3

--- a/solution.py
+++ b/solution.py
@@ -583,7 +583,7 @@
     att_t, att_out, att_all, conv_s, acc_v, acc_out, gate_out, gate_in, ext, rim_out, rim, sums, stats, stats_all,
     mine_ref,
     send_d, recv_d, send_r, recv_r, send_z, recv_z, local_sem, small_sem, rim_sem, x_sem,
-    part_sem, sp_send, sp_recv, fw_send, fw_recv, tp_send, tp_recv, out_send, out_recv, store_sem,
+    part_sem, sp_send, sp_recv, fw_send, fw_recv, tp_send, tp_recv, out_send, out_recv, store_sem, known,
 ):
     n_fs, n_sp, n_tp = sizes
     f = lax.axis_index("fs")
@@ -596,12 +596,21 @@
     twin = {"tp": 1 - t}
     even, odd = parity == 0, parity == 1
 
+    near_x = f + 1 - 2 * lax.rem(f, 2)
+    near_y = lax.rem(f + 2, 4)
+    far = lax.rem(near_x + 2, 4)
+    sources = [near_x, near_y]
+    has_below, has_above = s > 0, s < n_sp - 1
+
     barrier = pltpu.get_barrier_semaphore()
-    for axis, at, count in (("fs", f, n_fs), ("sp", s, n_sp), ("tp", t, n_tp)):
-        for k in range(1, count):
-            pl.semaphore_signal(
-                barrier, inc=1, device_id={axis: lax.rem(at + k, count)}, device_id_type=MESH_ID
-            )
+
+    def greet(device):
+        pl.semaphore_signal(barrier, inc=1, device_id=device, device_id_type=MESH_ID)
+
+    for device in (twin, {"fs": near_x}, {"fs": near_y}):
+        greet(device)
+    pl.when(has_below)(lambda: greet({"sp": s - 1}))
+    pl.when(has_above)(lambda: greet({"sp": s + 1}))
 
     slots = 3
     rows = x_hbm.shape[0]
@@ -632,11 +641,6 @@
     )
     theirs = x_all.at[1 - parity, slab, :]
     x_forward = remote(theirs, theirs, x_sem.at[3], x_sem.at[4], twin)
-
-    near_x = f + 1 - 2 * lax.rem(f, 2)
-    near_y = lax.rem(f + 2, 4)
-    far = lax.rem(near_x + 2, 4)
-    sources = [near_x, near_y]
 
     def job(a, shard, whole, swap=None, dim=0, first=0, count=None):
         depth, cols = shard.shape
@@ -693,6 +697,7 @@
     side = pl.ds(pl.multiple_of(parity * wide, 128), wide)
     half_rows = ho.shape[0] // 2
     last_rows = half_rows // 4
+    first_rows = half_rows * 10 // 8
 
     def swapping(lane, even_lacks, odd_lacks, *rest):
         shard, whole, *rest = rest
@@ -705,10 +710,10 @@
         [(even, qd, qd_all), (odd, md, md_all)],
         [(None, half_columns(ku), ku_all)], [(None, half_columns(vu), vu_all)],
         [(None, half_columns(qu), qu_all)],
-        swapping(0, 8, 8, ho, ho_all, 1, 0, half_rows),
+        swapping(0, 8, 8, ho, ho_all, 1, 0, first_rows),
         [(None, half_columns(cv), cv_all)], [(None, half_columns(cg), cg_all)],
-        swapping(1, 8, 8, ho, ho_all, 1, half_rows, half_rows),
-        swapping(2, 6, 4, co, co_all, 1, 0, half_rows),
+        swapping(1, 8, 8, ho, ho_all, 1, first_rows, 2 * half_rows - first_rows),
+        swapping(2, 5, 4, co, co_all, 1, 0, half_rows),
         [(None, co, co_all, None, 1, half_rows, half_rows - last_rows)],
         [(None, co, co_all, None, 1, 2 * half_rows - last_rows, last_rows)],
     ]
@@ -750,6 +755,16 @@
                 copy.start()
 
         each(a, go)
+
+    def swap_near(a):
+        def swap(parts):
+            for copy in parts[2][: len(sources)]:
+                copy.start()
+
+        if a in lanes:
+            each(a, swap)
+
+    begins = {0: [3], 1: [4], 2: [5], 3: [6], 5: [7], 6: [8], 7: [9], 8: [10]}
 
     def tick(a):
         def go(parts):
@@ -760,29 +775,34 @@
             for copy in parts[1]:
                 copy.start()
 
-        def swap(parts):
-            for copy in parts[2][: len(sources)]:
-                copy.start()
-
         sent(a - slots, 1)
         each(a, go)
-        begin_array(a + slots)
-        if a in lanes:
-            each(a, swap)
-
-    def complete(a):
+        for later in begins.get(a, ()):
+            begin_array(later)
+        swap_near(a)
+
+    def complete(a, which=slice(None)):
         def go(parts):
             with jax.named_scope(f"across_{a}"):
-                for copy in parts[4]:
+                for copy in parts[4][which]:
                     copy.wait_recv()
 
         each(a, go)
 
     with jax.named_scope("entry"):
-        pl.semaphore_wait(barrier, n_fs + n_sp + n_tp - 3)
+        pl.semaphore_wait(
+            barrier, 3 + has_below.astype(jnp.int32) + has_above.astype(jnp.int32)
+        )
     x_send.start()
     for a in range(slots):
         begin_array(a)
+
+    @pl.when(jnp.logical_and(has_below, has_above))
+    def _():
+        pl.semaphore_signal(
+            known.at[0], inc=1, device_id={"sp": s - 1}, device_id_type=MESH_ID
+        )
+
     with jax.named_scope("small_wait"):
         for r in range(0, len(small), slots):
             if r:
@@ -843,6 +863,11 @@
     norm_block(1 - parity)
     tick(2)
     finish_far(0)
+
+    @pl.when(s < n_sp - 2)
+    def _():
+        pl.semaphore_wait(known.at[0], 1)
+
 
     def project(weight, b):
         return jnp.dot(normed[b], weight[...], preferred_element_type=jnp.float32)
@@ -974,8 +999,6 @@
                 for copy in onward[d - 1][0]:
                     copy.wait_recv()
             forwards[d - 1].start()
-    tick(6)
-    finish_far(4)
     with jax.named_scope("query_wait"):
         query_copy.wait_recv()
     for b in range(2):
@@ -998,6 +1021,8 @@
                 forwards[d - 1].wait_recv()
     pl.loop(0, 2 * couple)(expand)
     q_t[...] = dot_heads(qu_all[...], qn_t[...])
+    tick(6)
+    finish_far(4)
     heads = qu.shape[1] // 2 // QK_DIM
     here = pl.ds(pl.multiple_of(2 * couple * rows, rows), 2 * rows)
     score_scale = QK_DIM ** (-0.5)
@@ -1041,10 +1066,10 @@
         att_t[vrow, :] = summed / total
 
     pl.loop(0, heads // 2)(head)
-    tick(7)
     finish_far(5)
     for b in range(2):
         acc_v[b] = project(cv_all, b)
+    tick(7)
     pl.loop(heads // 2, heads)(head)
     value_rows = heads * V_DIM
     own_rows = pl.ds(pl.multiple_of(parity * value_rows, value_rows), value_rows)
@@ -1056,7 +1081,6 @@
     att_out[...] = att_t[:, their_lanes].astype(jnp.bfloat16)
     att_across.start()
     att_all[own_rows, :] = att_t[:, own_lanes].astype(jnp.bfloat16)
-    tick(8)
     finish_far(6)
     opposite = pl.ds(pl.multiple_of((1 - parity) * wide, 128), wide)
     body_rows, halo = pl.ds(RIM, rows), pl.ds(0, RIM)
@@ -1102,7 +1126,7 @@
     def _():
         ext[body_rows, side] = upper.astype(jnp.float32)
 
-    tick(9)
+    tick(8)
 
     @pl.when(has_earlier)
     def _():
@@ -1117,15 +1141,21 @@
     tap_count = taps_ref.shape[0]
     block = 64
 
+    lead = RIM - (tap_count - 1)
+
     def convolve(c):
         cols = pl.ds(pl.multiple_of(c * 128, 128), 128)
         taps = taps_ref[:, cols].astype(jnp.float32)
         for r in range(0, rows, block):
             total = jnp.zeros((block, 128), jnp.float32)
-            for j in range(tap_count):
-                total = total + ext[
-                    pl.ds(r + RIM - (tap_count - 1) + j, block), cols
-                ] * taps[j : j + 1, :]
+            for shift in range(8):
+                height = block + (8 if shift else 0)
+                partial = jnp.zeros((height, 128), jnp.float32)
+                for offset in range(shift, RIM + 1, 8):
+                    if offset >= lead:
+                        tap = taps[offset - lead : offset - lead + 1, :]
+                        partial = partial + ext[pl.ds(r + offset - shift, height), cols] * tap
+                total = total + partial[shift : shift + block]
             sums[pl.ds(r, block), cols] = total
 
     tiles = wide // 128
@@ -1138,10 +1168,8 @@
     def _():
         ext[halo, opposite] = gate_in[halo, :].astype(jnp.float32)
 
+    pl.loop((1 - parity) * tiles, (2 - parity) * tiles)(convolve)
     finish_far(7)
-    pl.loop((1 - parity) * tiles, (2 - parity) * tiles)(convolve)
-    finish_far(8)
-    tick(10)
 
     @pl.loop(0, rows // part)
     def _(i):
@@ -1155,22 +1183,22 @@
         )
 
     stat_copy.start()
+    tick(9)
     with jax.named_scope("att_wait"):
         att_across.wait_recv()
     att = att_all[...].astype(jnp.float32).T.astype(jnp.bfloat16)
     span = ho.shape[1]
 
-    def gain_rows(left, weight, begin, size=half_rows, first=False):
-        band = slice(begin, begin + size)
-
-        @pl.loop(0, n_fs)
-        def _(i):
-            cols = pl.ds(pl.multiple_of(i * span, span), span)
-            product = jnp.dot(left[:, band], weight[band, cols], preferred_element_type=jnp.float32)
-            acc_out[:, cols] = product if first else acc_out[:, cols] + product
-
     complete(4)
-    gain_rows(att, ho_all, 0, first=True)
+
+    @pl.loop(0, n_fs)
+    def _(i):
+        cols = pl.ds(pl.multiple_of(i * span, span), span)
+        acc_out[:, cols] = jnp.dot(
+            att[:, :first_rows], ho_all[:first_rows, cols], preferred_element_type=jnp.float32
+        )
+
+    finish_far(8)
     with jax.named_scope("stat_wait"):
         stat_copy.wait_recv()
     channels = ext.shape[1] * n_tp
@@ -1189,13 +1217,7 @@
             shaped * cgain_ref[...] + cshift_ref[...]
         ).astype(jnp.bfloat16)
 
-    complete(7)
-    gain_rows(att, ho_all, half_rows)
-    complete(8)
-    gain_rows(conv_s, co_all, 0)
-    finish_far(9)
-    gain_rows(conv_s, co_all, half_rows, half_rows - last_rows)
-    rest = slice(2 * half_rows - last_rows, 2 * half_rows)
+    tick(10)
     outs, stores = [], []
     for i, owner in enumerate([f, near_x, near_y, far]):
         cols = pl.ds(pl.multiple_of(owner * span, span), span)
@@ -1205,14 +1227,18 @@
         stores.append(pltpu.make_async_copy(
             mine_ref.at[:, cols], mine_hbm.at[:, cols], store_sem.at[i]
         ))
+        if i == 1:
+            complete(7, slice(0, len(sources)))
+            complete(8, slice(0, len(sources)))
         if i == n_fs - 1:
+            finish_far(9)
             finish_far(last)
+            complete(7, slice(len(sources), None))
+            complete(8, slice(len(sources), None))
         mine_ref[:, cols] = (
             acc_out[:, cols]
-            + jnp.dot(
-                conv_s[:, rest], co_all[rest, cols],
-                preferred_element_type=jnp.float32,
-            )
+            + jnp.dot(att[:, first_rows:], ho_all[first_rows:, cols], preferred_element_type=jnp.float32)
+            + jnp.dot(conv_s[...], co_all[:, cols], preferred_element_type=jnp.float32)
         ).astype(jnp.bfloat16)
         outs[i].start()
         stores[i].start()
@@ -1363,6 +1389,7 @@
             dma((slots, 3)), dma((slots, 3)), dma((slots,)), dma((slots,)), dma((3,)),
             dma((5,)), dma((8,)), dma((spare, 2, 2)), dma((spare, 2)),
             dma((couples,)), dma((couples,)), dma((3,)), dma((3,)), dma((n_fs,)), dma((n_fs,)), dma((n_fs,)),
+            pltpu.SemaphoreType.REGULAR((1,)),
         ],
         compiler_params=pltpu.CompilerParams(
             collective_id=1, has_side_effects=True, vmem_limit_bytes=60 * 1024 * 1024

time: 79.1 us -> 73.6 us (0.930)
  Pallas kernels: 78.8 us -> 73.3 us
    pallas_call x1, Pallas kernels: 76.5 us -> 71 us  [fused_call(): pl.pallas_call(functools.partial(fused_kernel, sizes), out_shape=[jax.Sha...]
where the time goes in v4:
time: 73.6 us; the launch traced here: 73.4 us
  Pallas kernels  73.3 us (100%)
    pallas_call x1, Pallas kernels, fused_call(): pl.pallas_call(functools.partial(fused_kernel, sizes), out_shape=[jax.Sha...  71 us
    pallas_call x1, Pallas kernels, join(): pl.pallas_call(join_kernel, out_shape=jax.ShapeDtypeStruct(mine.shape, mi...  2.37 us

profile of v4, /device:TPU:0, one launch (start us, length us, event | category | flops | bytes accessed | tf_op | source)
XLA Modules:
  0.0 73.4 jit_solution(12870687430559818488)
XLA Ops:
  0.0 71.0 %shard_map.199 = (bf16[256,2048]{1,0:T(8,128)(2,1)}, bf16[256,2048]{1,0:T(8,128)(2,1)}) custom-call(bf16[256,2048]{1,0:T(8,128)(2,1)} %bitcast.10, f32[1,2048]{1,0:T(1,128)} %bitcast.12, bf16[32,2048]{1,0:T(8,128)(2,1)} %bitcast.11, bf16[31,512]{1,0:T(8,128)(2,1)} %taps_hbm.1, f32[1,512]{1,0:T(1,128)} %bitcast.14, f32[1,512]{1,0:T(1,128)} %bitcast.15, ...), custom_call_target="tpu_custom_call" | custom-call | tf_op jit(solution)/shard_map/pallas_call | solution.py:1357
  71.0 2.4 %shard_map.200 = bf16[256,2048]{1,0:T(8,128)(2,1)} custom-call(bf16[256,2048]{1,0:T(8,128)(2,1)} %get-tuple-element.7.mine_hbm, bf16[256,2048]{1,0:T(8,128)(2,1)} %get-tuple-element.8.other_hbm), custom_call_target="tpu_custom_call" | custom-call | tf_op jit(solution)/shard_map/pallas_call | solution.py:1318

commit v5 on v4

--- a/solution.py
+++ b/solution.py
@@ -574,16 +574,15 @@
     x_hbm, gain_hbm, rope_hbm, taps_hbm, cgain_hbm, cshift_hbm,
     lgain_hbm, mgain_hbm, qgain_hbm, kgain_hbm, cos_hbm, sin_hbm,
     qd, md, ku, vu, qu, cv, cg, ho, co,
-    mine_hbm, other_hbm,
+    mine_ref, other_ref,
     gain_ref, rope_ref, taps_ref, cgain_ref, cshift_ref,
     lgain_ref, mgain_ref, qgain_ref, kgain_ref, cos_ref, sin_ref,
     qd_all, md_all, ku_all, vu_all, qu_all, cv_all, cg_all, ho_all, co_all,
     x_all, normed, lq_all, lm_all, mem_all, rr_all, qn_t, q_t, k_t, v_t,
     turned, ropesq, qcol, kcol, bias, scores,
     att_t, att_out, att_all, conv_s, acc_v, acc_out, gate_out, gate_in, ext, rim_out, rim, sums, stats, stats_all,
-    mine_ref,
     send_d, recv_d, send_r, recv_r, send_z, recv_z, local_sem, small_sem, rim_sem, x_sem,
-    part_sem, sp_send, sp_recv, fw_send, fw_recv, tp_send, tp_recv, out_send, out_recv, store_sem, known,
+    part_sem, sp_send, sp_recv, fw_send, fw_recv, tp_send, tp_recv, out_send, out_recv, known,
 ):
     n_fs, n_sp, n_tp = sizes
     f = lax.axis_index("fs")
@@ -697,7 +696,7 @@
     side = pl.ds(pl.multiple_of(parity * wide, 128), wide)
     half_rows = ho.shape[0] // 2
     last_rows = half_rows // 4
-    first_rows = half_rows * 10 // 8
+    first_rows = half_rows * 12 // 8
 
     def swapping(lane, even_lacks, odd_lacks, *rest):
         shard, whole, *rest = rest
@@ -712,8 +711,8 @@
         [(None, half_columns(qu), qu_all)],
         swapping(0, 8, 8, ho, ho_all, 1, 0, first_rows),
         [(None, half_columns(cv), cv_all)], [(None, half_columns(cg), cg_all)],
-        swapping(1, 8, 8, ho, ho_all, 1, first_rows, 2 * half_rows - first_rows),
-        swapping(2, 5, 4, co, co_all, 1, 0, half_rows),
+        swapping(1, 8, 4, ho, ho_all, 1, first_rows, 2 * half_rows - first_rows),
+        swapping(2, 6, 2, co, co_all, 1, 0, half_rows),
         [(None, co, co_all, None, 1, half_rows, half_rows - last_rows)],
         [(None, co, co_all, None, 1, 2 * half_rows - last_rows, last_rows)],
     ]
@@ -1160,6 +1159,7 @@
 
     tiles = wide // 128
     pl.loop(parity * tiles, (parity + 1) * tiles)(convolve)
+    pl.when(odd)(lambda: tick(9))
     with jax.named_scope("gate_wait"):
         gate_across.wait_recv()
     ext[body_rows, opposite] = gate_in[body_rows, :].astype(jnp.float32)
@@ -1183,7 +1183,7 @@
         )
 
     stat_copy.start()
-    tick(9)
+    pl.when(even)(lambda: tick(9))
     with jax.named_scope("att_wait"):
         att_across.wait_recv()
     att = att_all[...].astype(jnp.float32).T.astype(jnp.bfloat16)
@@ -1218,14 +1218,11 @@
         ).astype(jnp.bfloat16)
 
     tick(10)
-    outs, stores = [], []
+    outs = []
     for i, owner in enumerate([f, near_x, near_y, far]):
         cols = pl.ds(pl.multiple_of(owner * span, span), span)
         outs.append(remote(
-            mine_ref.at[:, cols], other_hbm.at[:, cols], out_send.at[i], out_recv.at[i], twin
-        ))
-        stores.append(pltpu.make_async_copy(
-            mine_ref.at[:, cols], mine_hbm.at[:, cols], store_sem.at[i]
+            mine_ref.at[:, cols], other_ref.at[:, cols], out_send.at[i], out_recv.at[i], twin
         ))
         if i == 1:
             complete(7, slice(0, len(sources)))
@@ -1241,7 +1238,6 @@
             + jnp.dot(conv_s[...], co_all[:, cols], preferred_element_type=jnp.float32)
         ).astype(jnp.bfloat16)
         outs[i].start()
-        stores[i].start()
 
     for a in range(last + 1 - slots, last + 1):
         sent(a, 0)
@@ -1277,52 +1273,8 @@
         later_rim.wait_send()
 
     with jax.named_scope("out_wait"):
-        for copy in outs + stores:
+        for copy in outs:
             copy.wait()
-
-
-def join_kernel(mine_hbm, other_hbm, out_hbm, mine, other, whole, loads, stores):
-    rows = mine.shape[0]
-    pieces = loads.shape[0]
-    step = rows // pieces
-
-    def copies(i):
-        at = pl.ds(i * step, step)
-        return (
-            pltpu.make_async_copy(mine_hbm.at[at, :], mine.at[at, :], loads.at[i, 0]),
-            pltpu.make_async_copy(other_hbm.at[at, :], other.at[at, :], loads.at[i, 1]),
-            pltpu.make_async_copy(whole.at[at, :], out_hbm.at[at, :], stores.at[i]),
-        )
-
-    plan = [copies(i) for i in range(pieces)]
-    for one, two, _ in plan:
-        one.start()
-        two.start()
-    for i, (one, two, back) in enumerate(plan):
-        one.wait()
-        two.wait()
-        at = pl.ds(i * step, step)
-        whole[at, :] = (
-            mine[at, :].astype(jnp.float32) + other[at, :].astype(jnp.float32)
-        ).astype(jnp.bfloat16)
-        back.start()
-    for _, _, back in plan:
-        back.wait()
-
-
-def join(mine, other):
-    pieces = 4
-    buffer = pltpu.VMEM(mine.shape, mine.dtype)
-    dma = pltpu.SemaphoreType.DMA
-    hbm = pl.BlockSpec(memory_space=pl.ANY)
-    return pl.pallas_call(
-        join_kernel,
-        out_shape=jax.ShapeDtypeStruct(mine.shape, mine.dtype),
-        in_specs=[hbm] * 2,
-        out_specs=hbm,
-        scratch_shapes=[buffer] * 3 + [dma((pieces, 2)), dma((pieces,))],
-        compiler_params=pltpu.CompilerParams(vmem_limit_bytes=60 * 1024 * 1024),
-    )(mine, other)
 
 
 def fused_call(
@@ -1358,7 +1310,7 @@
         functools.partial(fused_kernel, sizes),
         out_shape=[jax.ShapeDtypeStruct((rows, ho.shape[1] * n_fs), bf16)] * 2,
         in_specs=[hbm] * 21,
-        out_specs=[hbm] * 2,
+        out_specs=[pl.BlockSpec(memory_space=pltpu.VMEM)] * 2,
         scratch_shapes=[scratch(*a.shape, dtype=a.dtype) for a in small] + [
             scratch(*whole(qd), dtype=bf16), scratch(*whole(md), dtype=bf16),
             scratch(*whole(ku, 0, 2), dtype=bf16), scratch(*whole(vu, 0, 2), dtype=bf16),
@@ -1384,17 +1336,19 @@
             scratch(rows + RIM, channels), scratch(RIM, channels // 2, dtype=bf16),
             scratch(2, RIM, channels // 2, dtype=bf16), scratch(rows, channels),
             scratch(2 * rows, 128), scratch(2 * rows, 128),
-            scratch(rows, ho.shape[1] * n_fs, dtype=bf16),
             dma((slots, 2)), dma((count, 2)), dma((slots, 2)), dma((count, 2)),
             dma((slots, 3)), dma((slots, 3)), dma((slots,)), dma((slots,)), dma((3,)),
             dma((5,)), dma((8,)), dma((spare, 2, 2)), dma((spare, 2)),
-            dma((couples,)), dma((couples,)), dma((3,)), dma((3,)), dma((n_fs,)), dma((n_fs,)), dma((n_fs,)),
+            dma((couples,)), dma((couples,)), dma((3,)), dma((3,)), dma((n_fs,)), dma((n_fs,)),
             pltpu.SemaphoreType.REGULAR((1,)),
         ],
         compiler_params=pltpu.CompilerParams(
-            collective_id=1, has_side_effects=True, vmem_limit_bytes=60 * 1024 * 1024
+            collective_id=1, has_side_effects=True, vmem_limit_bytes=40 * 1024 * 1024
         ),
-    )(x, *small, qd, md, ku, vu, qu, cv, cg, ho, co)
+    )(*[
+        pltpu.with_memory_space_constraint(a, pltpu.HBM)
+        for a in (x, *small, qd, md, ku, vu, qu, cv, cg, ho, co)
+    ])
 
 
 def fused_local(
@@ -1409,7 +1363,7 @@
         query_down, memory_down, conv_value, conv_gate,
         query_up, key_up, value_up, heads_out, conv_out,
     )
-    return join(mine, other)[None]
+    return (mine.astype(jnp.float32) + other.astype(jnp.float32)).astype(jnp.bfloat16)[None]
 
 
 def solution(mesh):

time: 73.6 us -> 71.7 us (0.974)
  Pallas kernels: 73.3 us -> 70.1 us
  other arithmetic: 0 us -> 1.36 us
    pallas_call x1 -> x0, Pallas kernels: 2.37 us -> none  [join(): pl.pallas_call(join_kernel, out_shape=jax.ShapeDtypeStruct(mine.shape, mi...]
    broadcast_in_dim x0 -> x1, other arithmetic: none -> 1.36 us  [fused_local(): (mine.astype(jnp.float32) + other.astype(jnp.float32)).astype(jnp.bfloat16)]
    pallas_call x1, Pallas kernels: 71 us -> 70.1 us  [fused_call(): pl.pallas_call(functools.partial(fused_kernel, sizes), out_shape=[jax.Sha...]
where the time goes in v5:
time: 71.7 us; the launch traced here: 71.5 us
  Pallas kernels  70.1 us (98%)
  other arithmetic  1.36 us (2%)
    pallas_call x1, Pallas kernels, fused_call(): pl.pallas_call(functools.partial(fused_kernel, sizes), out_shape=[jax.Sha...  70.1 us

profile of v5, /device:TPU:0, one launch (start us, length us, event | category | flops | bytes accessed | tf_op | source)
XLA Modules:
  0.0 71.5 jit_solution(7321393785772350722)
XLA Ops:
  0.0 70.1 %shard_map.199 = (bf16[256,2048]{1,0:T(8,128)(2,1)S(1)}, bf16[256,2048]{1,0:T(8,128)(2,1)S(1)}) custom-call(bf16[256,2048]{1,0:T(8,128)(2,1)} %bitcast.11, f32[1,2048]{1,0:T(1,128)} %bitcast.13, bf16[32,2048]{1,0:T(8,128)(2,1)} %bitcast.12, bf16[31,512]{1,0:T(8,128)(2,1)} %taps_hbm.1, f32[1,512]{1,0:T(1,128)} %bitcast.15, f32[1,512]{1,0:T(1,128)} %bitcast.16, ...), custom_call_target="tpu_custom_call" | custom-call | tf_op jit(solution)/shard_map/pallas_call | solution.py:1309
  70.1 1.4 %fusion = bf16[1,256,2048]{2,1,0:T(8,128)(2,1)} fusion(bf16[256,2048]{1,0:T(8,128)(2,1)S(1)} %get-tuple-element.8, bf16[256,2048]{1,0:T(8,128)(2,1)S(1)} %get-tuple-element.7), kind=kLoop, calls=%fused_computation.1 | loop fusion | flops 2097152 | bytes 3145728 | tf_op jit(solution)/shard_map/broadcast_in_dim | solution.py:1366

commit v6 on v5

--- a/solution.py
+++ b/solution.py
@@ -696,7 +696,7 @@
     side = pl.ds(pl.multiple_of(parity * wide, 128), wide)
     half_rows = ho.shape[0] // 2
     last_rows = half_rows // 4
-    first_rows = half_rows * 12 // 8
+    first_rows = half_rows * 14 // 8
 
     def swapping(lane, even_lacks, odd_lacks, *rest):
         shard, whole, *rest = rest
@@ -708,11 +708,11 @@
     plan = [
         [(even, qd, qd_all), (odd, md, md_all)],
         [(None, half_columns(ku), ku_all)], [(None, half_columns(vu), vu_all)],
+        swapping(0, 8, 8, ho, ho_all, 1, 0, first_rows),
         [(None, half_columns(qu), qu_all)],
-        swapping(0, 8, 8, ho, ho_all, 1, 0, first_rows),
         [(None, half_columns(cv), cv_all)], [(None, half_columns(cg), cg_all)],
         swapping(1, 8, 4, ho, ho_all, 1, first_rows, 2 * half_rows - first_rows),
-        swapping(2, 6, 2, co, co_all, 1, 0, half_rows),
+        swapping(2, 8, 2, co, co_all, 1, 0, half_rows),
         [(None, co, co_all, None, 1, half_rows, half_rows - last_rows)],
         [(None, co, co_all, None, 1, 2 * half_rows - last_rows, last_rows)],
     ]
@@ -1019,9 +1019,9 @@
             with jax.named_scope(f"forward_{d}"):
                 forwards[d - 1].wait_recv()
     pl.loop(0, 2 * couple)(expand)
-    q_t[...] = dot_heads(qu_all[...], qn_t[...])
     tick(6)
     finish_far(4)
+    q_t[...] = dot_heads(qu_all[...], qn_t[...])
     heads = qu.shape[1] // 2 // QK_DIM
     here = pl.ds(pl.multiple_of(2 * couple * rows, rows), 2 * rows)
     score_scale = QK_DIM ** (-0.5)
@@ -1189,7 +1189,7 @@
     att = att_all[...].astype(jnp.float32).T.astype(jnp.bfloat16)
     span = ho.shape[1]
 
-    complete(4)
+    complete(3)
 
     @pl.loop(0, n_fs)
     def _(i):

time: 71.7 us -> 70.6 us (0.985)
  Pallas kernels: 70.1 us -> 69 us
    pallas_call x1, Pallas kernels: 70.1 us -> 69 us  [fused_call(): pl.pallas_call(functools.partial(fused_kernel, sizes), out_shape=[jax.Sha...]
where the time goes in v6:
time: 70.6 us; the launch traced here: 70.4 us
  Pallas kernels  69 us (98%)
  other arithmetic  1.36 us (2%)
    pallas_call x1, Pallas kernels, fused_call(): pl.pallas_call(functools.partial(fused_kernel, sizes), out_shape=[jax.Sha...  69 us

profile of v6, /device:TPU:0, one launch (start us, length us, event | category | flops | bytes accessed | tf_op | source)
XLA Modules:
  0.0 70.4 jit_solution(11857641088489130071)
XLA Ops:
  0.0 69.0 %shard_map.199 = (bf16[256,2048]{1,0:T(8,128)(2,1)S(1)}, bf16[256,2048]{1,0:T(8,128)(2,1)S(1)}) custom-call(bf16[256,2048]{1,0:T(8,128)(2,1)} %bitcast.11, f32[1,2048]{1,0:T(1,128)} %bitcast.13, bf16[32,2048]{1,0:T(8,128)(2,1)} %bitcast.12, bf16[31,512]{1,0:T(8,128)(2,1)} %taps_hbm.1, f32[1,512]{1,0:T(1,128)} %bitcast.15, f32[1,512]{1,0:T(1,128)} %bitcast.16, ...), custom_call_target="tpu_custom_call" | custom-call | tf_op jit(solution)/shard_map/pallas_call | solution.py:1309
  69.0 1.4 %fusion = bf16[1,256,2048]{2,1,0:T(8,128)(2,1)} fusion(bf16[256,2048]{1,0:T(8,128)(2,1)S(1)} %get-tuple-element.8, bf16[256,2048]{1,0:T(8,128)(2,1)S(1)} %get-tuple-element.7), kind=kLoop, calls=%fused_computation.1 | loop fusion | flops 2097152 | bytes 3145728 | tf_op jit(solution)/shard_map/broadcast_in_dim | solution.py:1366

commit v7 on v6

--- a/solution.py
+++ b/solution.py
@@ -1219,8 +1219,10 @@
 
     tick(10)
     outs = []
-    for i, owner in enumerate([f, near_x, near_y, far]):
-        cols = pl.ds(pl.multiple_of(owner * span, span), span)
+    pieces = [(owner, 0, span) for owner in (f, near_x, near_y)]
+    pieces += [(far, 0, span // 2), (far, span // 2, span // 2)]
+    for i, (owner, begin, width) in enumerate(pieces):
+        cols = pl.ds(pl.multiple_of(owner * span + begin, 128), width)
         outs.append(remote(
             mine_ref.at[:, cols], other_ref.at[:, cols], out_send.at[i], out_recv.at[i], twin
         ))
@@ -1339,7 +1341,7 @@
             dma((slots, 2)), dma((count, 2)), dma((slots, 2)), dma((count, 2)),
             dma((slots, 3)), dma((slots, 3)), dma((slots,)), dma((slots,)), dma((3,)),
             dma((5,)), dma((8,)), dma((spare, 2, 2)), dma((spare, 2)),
-            dma((couples,)), dma((couples,)), dma((3,)), dma((3,)), dma((n_fs,)), dma((n_fs,)),
+            dma((couples,)), dma((couples,)), dma((3,)), dma((3,)), dma((n_fs + 1,)), dma((n_fs + 1,)),
             pltpu.SemaphoreType.REGULAR((1,)),
         ],
         compiler_params=pltpu.CompilerParams(

time: 70.6 us -> 70.8 us (level)
  no operation moved by 1% of the time
where the time goes in v7:
time: 70.8 us; the launch traced here: 70.6 us
  Pallas kernels  69.2 us (98%)
  other arithmetic  1.36 us (2%)
    pallas_call x1, Pallas kernels, fused_call(): pl.pallas_call(functools.partial(fused_kernel, sizes), out_shape=[jax.Sha...  69.2 us

profile of v7, /device:TPU:0, one launch (start us, length us, event | category | flops | bytes accessed | tf_op | source)
XLA Modules:
  0.0 70.6 jit_solution(14266182855307455438)
XLA Ops:
  0.0 69.2 %shard_map.199 = (bf16[256,2048]{1,0:T(8,128)(2,1)S(1)}, bf16[256,2048]{1,0:T(8,128)(2,1)S(1)}) custom-call(bf16[256,2048]{1,0:T(8,128)(2,1)} %bitcast.11, f32[1,2048]{1,0:T(1,128)} %bitcast.13, bf16[32,2048]{1,0:T(8,128)(2,1)} %bitcast.12, bf16[31,512]{1,0:T(8,128)(2,1)} %taps_hbm.1, f32[1,512]{1,0:T(1,128)} %bitcast.15, f32[1,512]{1,0:T(1,128)} %bitcast.16, ...), custom_call_target="tpu_custom_call" | custom-call | tf_op jit(solution)/shard_map/pallas_call | solution.py:1311
  69.2 1.4 %fusion = bf16[1,256,2048]{2,1,0:T(8,128)(2,1)} fusion(bf16[256,2048]{1,0:T(8,128)(2,1)S(1)} %get-tuple-element.8, bf16[256,2048]{1,0:T(8,128)(2,1)S(1)} %get-tuple-element.7), kind=kLoop, calls=%fused_computation.1 | loop fusion | flops 2097152 | bytes 3145728 | tf_op jit(solution)/shard_map/broadcast_in_dim | solution.py:1368
